TPU v7x, 256 devices: a whole 4x4x8 slice. The times are simulated.
256 devices in a mesh: fs: 16 (over y, x), tp: 16 (over z, core).
Axes of the slice: x: 4, y: 4, z: 8, core: 2. Of those that a mesh axis runs over, the one named last changes fastest.
Arguments:
- tokens: bfloat16 [32768, 2048], P(('fs', 'tp')), may hold values from -6 to 6
- norm_gain: float32 [2048], replicated, may hold values from 0.1 to 1.9
- gate_weight: bfloat16 [2048, 5632], P('fs', 'tp'), may hold values from -0.125 to 0.125
- up_weight: bfloat16 [2048, 5632], P('fs', 'tp'), may hold values from -0.125 to 0.125
- down_weight: bfloat16 [5632, 2048], P('tp', 'fs'), may hold values from -0.078125 to 0.078125
Outputs:
- mixed: bfloat16 [32768, 2048], P(('fs', 'tp'))
All inputs are finite; a program needn't handle non-finite values.
Results may differ from a plain program's by a relative error of at most 0.0065.
Values may be sent and summed in bfloat16 or wider, within the bound.
No kernel may reach another device: no remote copies, remote signals or barrier semaphores. Data moves between devices by JAX's collectives and lax.ppermute only.
A program may use at most 128 MiB of HBM per device.

v0:
```python
import functools

import jax
import jax.numpy as jnp
from jax import lax
from jax.experimental import pallas as pl
from jax.experimental.pallas import tpu as pltpu
from jax.sharding import Mesh, PartitionSpec as P


eps_floor = 0.05
X, Y, Z = 4, 4, 8
AXES = ("y", "x", "z", "c")
LANES = 128
f32, bf16 = jnp.float32, jnp.bfloat16


def place(y, x, z, c):
    return ((y * X + x) * Z + z) * 2 + c


ROWS = [[place(y, x, z, 0) for x in range(X)] for y in range(Y) for z in range(Z)]
ROWS += [[place(y, x, z, 1) for y in range(Y)] for x in range(X) for z in range(Z)]
WHOLE = pl.BlockSpec(memory_space=pltpu.VMEM)
FULL = pltpu.CompilerParams(vmem_limit_bytes=67_000_000)
SMALL = pltpu.CompilerParams(vmem_limit_bytes=12 << 20)


def onward(x, by):
    pairs = [(2 * z + c, 2 * ((z + (by if c == 0 else -by)) % Z) + c) for z in range(Z) for c in range(2)]
    return lax.ppermute(x, ("z", "c"), pairs)


def along_column(x, by):
    flat = lambda y, x, c: (y % Y * X + x % X) * 2 + c
    pairs = [(flat(j, i, 0), flat(j + by, i, 0)) for j in range(Y) for i in range(X)]
    pairs += [(flat(j, i, 1), flat(j, i + by, 1)) for j in range(Y) for i in range(X)]
    return lax.ppermute(x, ("y", "x", "c"), pairs)


def swap(x):
    return lax.ppermute(x, "c", [(0, 1), (1, 0)])


def from_four(copies, groups):
    return lax.all_to_all(copies, AXES, 0, 0, axis_index_groups=groups, tiled=True)


def open_body(tokens_in, gain_in, gate_in, upper_in, down_in, normed_out, out, tokens, gain, down, normed, packed, sems):
    units = gate_in.shape[0]
    ends = [(tokens_in, tokens), (gain_in, gain), (down_in, down), (gate_in, packed.at[:units])]
    ends.append((upper_in, packed.at[units : 2 * units]))
    into = [pltpu.make_async_copy(*e, sems.at[i]) for i, e in enumerate(ends)]
    for c in into:
        c.start()
    for c in into[:2]:
        c.wait()
    values = tokens[...].astype(f32)
    factor = lax.rsqrt(jnp.mean(values * values, axis=-1, keepdims=True) + eps_floor)
    normed[...] = (values * factor * gain[...]).T.astype(bf16)
    copies = [pltpu.make_async_copy(normed, normed_out, sems.at[5])]
    copies[0].start()
    for c in into[2:]:
        c.wait()
    for at in range(0, units, LANES):
        n = min(LANES, units - at)
        rows = slice(2 * units + at, 2 * units + at + LANES)
        packed[rows, :n] = down[at : at + n].T
        if n < LANES:
            packed[rows, n:] = jnp.zeros((LANES, LANES - n), bf16)
    for k in range(4):
        copies.append(pltpu.make_async_copy(packed, out.at[k], sems.at[6 + k]))
        copies[-1].start()
    for c in copies:
        c.wait()


def opening(tokens, gain, gate, upper, down):
    units, (n, features) = gate.shape[0], tokens.shape
    shape = (2 * units + pl.cdiv(units, LANES) * LANES, LANES)
    remote = pl.BlockSpec(memory_space=pltpu.HBM)
    return pl.pallas_call(
        open_body,
        out_shape=[jax.ShapeDtypeStruct((features, n), bf16), jax.ShapeDtypeStruct((4, *shape), bf16)],
        in_specs=[remote] * 5,
        out_specs=[remote] * 2,
        scratch_shapes=[
            pltpu.VMEM(tokens.shape, bf16),
            pltpu.VMEM((1, features), f32),
            pltpu.VMEM(down.shape, bf16),
            pltpu.VMEM((features, n), bf16),
            pltpu.VMEM(shape, bf16),
            pltpu.SemaphoreType.DMA((10,)),
        ],
        compiler_params=FULL,
        name="opening",
    )(tokens, gain[None], gate, upper, down)


def spread_body(blocks, whole, *halves):
    n = halves[0].shape[0]
    for i, out in enumerate(halves):
        for k in range(4):
            part = blocks[k, n * i : n * (i + 1)]
            out[:, LANES * k : LANES * (k + 1)] = part
            whole[n * i : n * (i + 1), LANES * k : LANES * (k + 1)] = part


def spread(blocks):
    return pl.pallas_call(
        spread_body,
        out_shape=[jax.ShapeDtypeStruct((blocks.shape[1] // n, 4 * LANES), bf16) for n in (1, 2, 2)],
        in_specs=[WHOLE],
        out_specs=[WHOLE] * 3,
        compiler_params=SMALL,
        name="spread",
    )(blocks)


PARTS = ((0, None), (3, 0), (3, 1), (1, 0), (1, 1), (2, 0), (2, 1))


def hold_body(parts, sides, *refs):
    n, places, refs = len(parts), refs[:sides], refs[sides:]
    outs, sems = refs[-1 - sides : -1], refs[-1]
    half, copies = outs[0].shape[1] // 2, []
    for s, out in enumerate(outs):
        for i, (by, h) in enumerate(parts):
            at = (places[s][0] + by) % 4
            end = out.at[at] if h is None else out.at[at, half * h : half * (h + 1)]
            copies.append(pltpu.make_async_copy(refs[n * s + i], end, sems.at[n * s + i]))
    for c in copies:
        c.start()
    for c in copies:
        c.wait()


def hold(places, parts, blocks, shape, so_far=None):
    n, sides = len(blocks), len(places)
    more = [] if so_far is None else [so_far]
    remote = pl.BlockSpec(memory_space=pltpu.HBM)
    return pl.pallas_call(
        functools.partial(hold_body, parts, sides),
        out_shape=[jax.ShapeDtypeStruct(shape, bf16)] * sides,
        in_specs=[pl.BlockSpec(memory_space=pltpu.SMEM)] * sides + [remote] * n + [WHOLE] * len(more),
        out_specs=[WHOLE] * sides,
        input_output_aliases={n + sides: 0} if more else {},
        scratch_shapes=[pltpu.SemaphoreType.DMA((n,))],
        compiler_params=SMALL,
        name="hold",
    )(*places, *blocks, *more)


def order(core, b, w):
    return jnp.where(core == w, b, (b % 4) * 4 + b // 4)


def half_hidden(core, w, units, pieces, weights, turned):
    m, depth = pieces[0].shape[1], weights.shape[2]
    for b in range(turned.shape[0] // LANES):
        at = pl.ds(pl.multiple_of(order(core, b, w) * LANES, LANES), LANES)
        for i, piece in enumerate(pieces):
            turned[LANES * b : LANES * (b + 1), m * i : m * (i + 1)] = piece[at, :]
    both = jnp.dot(weights[0, : 2 * units], turned[:depth], preferred_element_type=f32)
    for k in range(1, 4):
        both += jnp.dot(weights[k, : 2 * units], turned[depth * k : depth * (k + 1)], preferred_element_type=f32)
    gate, upper = both[:units], both[units:]
    return (gate / (1.0 + jnp.exp(-gate)) * upper).astype(bf16)


def begin_body(n, units, core_ref, *refs):
    pieces, weights, out, turned = refs[:n], refs[n], refs[n + 1], refs[n + 2]
    out[...] = half_hidden(core_ref[0], 0, units, pieces, weights, turned)


def finish_body(n, units, core_ref, *refs):
    pieces, weights, first = refs[:n], refs[n : n + 2], refs[n + 2]
    outs, turned, held = refs[n + 3 : 2 * n + 3], refs[2 * n + 3], refs[2 * n + 4]
    core, m = core_ref[0], pieces[0].shape[1]
    hidden = first, held
    held[...] = half_hidden(core, 1, units, pieces, weights[1], turned)

    def four(group, carry):
        for j in range(4):
            b = group * 4 + j
            part = 0.0
            for w in (0, 1):
                at = order(core, b, w)
                lanes = pl.ds(pl.multiple_of(at % 4 * LANES, LANES), LANES)
                tiles = [weights[w][at // 4, r : r + LANES, lanes] for r in range(2 * units, weights[w].shape[1], LANES)]
                part += jnp.dot(jnp.concatenate(tiles, axis=1)[:, :units], hidden[w][...], preferred_element_type=f32)
            rows = pl.ds(pl.multiple_of(b * LANES, LANES), LANES)
            for i in range(n):
                outs[i][rows, :] = part[:, m * i : m * (i + 1)].astype(outs[i].dtype)
        return carry

    lax.fori_loop(0, turned.shape[0] // LANES // 4, four, 0)


def call(body, units, core, pieces, rest, out_shape):
    n, (features, m) = len(pieces), pieces[0].shape
    return pl.pallas_call(
        functools.partial(body, n, units),
        out_shape=out_shape,
        in_specs=[pl.BlockSpec(memory_space=pltpu.SMEM)] + [WHOLE] * (n + len(rest)),
        out_specs=jax.tree.map(lambda _: WHOLE, out_shape),
        scratch_shapes=[pltpu.VMEM((features, n * m), bf16), pltpu.VMEM((units, n * m), bf16)],
        compiler_params=pltpu.CompilerParams(vmem_limit_bytes=18 << 20),
    )(core, *pieces, *rest)


def begin(units, core, pieces, weights):
    n, m = len(pieces), pieces[0].shape[1]
    return call(begin_body, units, core, pieces, [weights], jax.ShapeDtypeStruct((units, n * m), bf16))


def finish(units, core, pieces, weights, first, dtype):
    out_shape = [jax.ShapeDtypeStruct(p.shape, dtype) for p in pieces]
    return call(finish_body, units, core, pieces, [*weights, first], out_shape)


def close_body(own, first, second, out):
    out[...] = (own[...] + first[...].astype(f32) + second[...].astype(f32)).T.astype(bf16)


def close(own, first, second):
    return pl.pallas_call(
        close_body,
        out_shape=jax.ShapeDtypeStruct(own.shape[::-1], bf16),
        in_specs=[WHOLE] * 3,
        out_specs=WHOLE,
        compiler_params=SMALL,
        name="close",
    )(own, first, second)


def local(tokens, norm_gain, gate_weight, up_weight, down_weight):
    core = lax.axis_index("c").astype(jnp.int32)[None]
    normed, packed = opening(tokens, norm_gain, gate_weight.T, up_weight.T, down_weight)

    own, mate = {0: normed}, {0: swap(normed)}
    for d in (1, 2, 3, 4):
        own[d] = onward(own[d - 1], 1)
        if d < 4:
            mate[d] = onward(mate[d - 1], 1)

    rows = from_four(packed, ROWS)
    here, top, bottom = spread(rows)
    before_top = along_column(top, 1)
    after_bottom = along_column(bottom, -1)
    before_bottom = along_column(bottom, 1)
    after_top = along_column(top, -1)
    far_top = along_column(before_top, 1)
    far_bottom = along_column(after_bottom, -1)
    blocks = here, before_top, before_bottom, after_top, after_bottom, far_top, far_bottom
    others = []
    for b in blocks:
        others.append(swap(b))
    row, column = lax.axis_index("y").astype(jnp.int32)[None], lax.axis_index("x").astype(jnp.int32)[None]
    first = core == 0
    mine, other = jnp.where(first, row, column), jnp.where(first, column, row)
    shape = (4, *here.shape)
    columns, others_columns = hold([mine, other], PARTS[:5], [*blocks[:5], *others[:5]], shape)
    (columns,) = hold([mine], PARTS[5:], blocks[5:], shape, columns)
    (others_columns,) = hold([other], PARTS[5:], others[5:], shape, others_columns)
    weights = columns, others_columns

    units = down_weight.shape[0]
    groups = [(own[4], mate[3]), (own[3], mate[2]), (own[2], mate[1]), (own[1],), (own[0],)]
    firsts = []
    for g in groups:
        firsts.append(begin(units, core, g, columns))
    shares = []
    for i, (g, f) in enumerate(zip(groups, firsts)):
        shares.append(finish(units, core, g, weights, f, f32 if i else bf16))
    (own4, mate3), (own3, mate2), (own2, mate1), (own1,), (own0,) = shares

    def send(x):
        return onward(x.astype(bf16), -1)

    got_own = send(own4)
    got_mate = send(mate3)
    got_own = send(got_own.astype(f32) + own3)
    got_mate = send(got_mate.astype(f32) + mate2)
    got_own = send(got_own.astype(f32) + own2)
    got_mate = send(got_mate.astype(f32) + mate1)
    got_own = send(got_own.astype(f32) + own1)
    return close(own0, got_own, swap(got_mate))


def solution(mesh):
    fine = Mesh(mesh.devices.reshape(Y, X, Z, 2), AXES)
    fs, tp = ("y", "x"), ("z", "c")

    return jax.shard_map(
        local,
        mesh=fine,
        in_specs=(P(fs + tp, None), P(), P(fs, tp), P(fs, tp), P(tp, fs)),
        out_specs=P(fs + tp, None),
        check_vma=False,
    )
```

profile of v0, /device:TPU:2, one launch (start us, length us, event | category | flops | bytes accessed | tf_op | source)
XLA Modules:
  0.0 126.3 jit_solution(4235621288936435052)
XLA Ops:
  0.0 2.6 %opening.1 = (bf16[2048,128]{1,0:T(8,128)(2,1)}, bf16[4,1088,128]{2,1,0:T(8,128)(2,1)}) custom-call(bf16[128,2048]{1,0:T(8,128)(2,1)} %tokens_in.1, f32[1,2048]{1,0:T(1,128)} %bitcast.8, bf16[352,128]{1,0:T(8,128)(2,1)} %bitcast.6, bf16[352,128]{1,0:T(8,128)(2,1)} %bitcast.7, bf16[352,128]{1,0:T(8,128)(2,1)} %down_in.1), custom_call_target="tpu_custom_call" | custom-call | tf_op jit(solution)/shard_map/opening/pallas_call | solution.py:82
  2.7 5.7 %all-to-all-start = ((bf16[4,1088,128]{2,1,0:T(8,128)(2,1)}), bf16[4,1088,128]{2,1,0:T(8,128)(2,1)S(1)}, u32[]{:S(2)}, u32[]{:S(2)}) async-start(bf16[4,1088,128]{2,1,0:T(8,128)(2,1)} %get-tuple-element.19), calls=%async_computation | async-start | bytes 2228224 | tf_op jit(solution)/shard_map/all_to_all | solution.py:46
  8.4 1.0 collective-permute-start.13
  9.4 2.9 %collective-permute-start.17 = (bf16[2048,128]{1,0:T(8,128)(2,1)}, bf16[2048,128]{1,0:T(8,128)(2,1)S(1)}, u32[]{:S(2)}, u32[]{:S(2)}) collective-permute-start(bf16[2048,128]{1,0:T(8,128)(2,1)} %get-tuple-element.18.refs_0_), channel_id=1, source_target_pairs={{0,1},{1,0},{2,3},{3,2},{4,5},{5,4},{6,7},{7,6},{8,9},{9,8},{10,11... | collective-permute-start | bytes 1572872 | tf_op jit(solution)/shard_map/ppermute | solution.py:42
  12.3 8.5 %collective-permute-done.13.refs_0_ = bf16[2048,128]{1,0:T(8,128)(2,1)S(1)} collective-permute-done((bf16[2048,128]{1,0:T(8,128)(2,1)}, bf16[2048,128]{1,0:T(8,128)(2,1)S(1)}, u32[]{:S(2)}, u32[]{:S(2)}) %collective-permute-start.13) | collective-permute-done | bytes 524320 | tf_op jit(solution)/shard_map/ppermute | solution.py:31
  21.0 1.2 collective-permute-start.6
  22.2 1.0 copy-done.3
  23.3 1.7 %collective-permute-start = (bf16[544,512]{1,0:T(8,128)(2,1)S(1)}, bf16[544,512]{1,0:T(8,128)(2,1)S(1)}, u32[]{:S(2)}, u32[]{:S(2)}) collective-permute-start(bf16[544,512]{1,0:T(8,128)(2,1)S(1)} %get-tuple-element.20), channel_id=1, source_target_pairs={{0,64},{16,80},{32,96},{48,112},{64,128},{80,144},{96,160},{112,17... | collective-permute-start | bytes 1671176 | tf_op jit(solution)/shard_map/ppermute | solution.py:38
  25.0 1.5 %collective-permute-start.2 = (bf16[544,512]{1,0:T(8,128)(2,1)S(1)}, bf16[544,512]{1,0:T(8,128)(2,1)}, u32[]{:S(2)}, u32[]{:S(2)}) collective-permute-start(bf16[544,512]{1,0:T(8,128)(2,1)S(1)} %get-tuple-element.21), channel_id=1, source_target_pairs={{0,192},{16,208},{32,224},{48,240},{64,0},{80,16},{96,32},{112,48}... | collective-permute-start | bytes 1671176 | tf_op jit(solution)/shard_map/ppermute | solution.py:38
  26.5 4.6 %collective-permute-done.14.refs_0_ = bf16[2048,128]{1,0:T(8,128)(2,1)S(1)} collective-permute-done((bf16[2048,128]{1,0:T(8,128)(2,1)S(1)}, bf16[2048,128]{1,0:T(8,128)(2,1)S(1)}, u32[]{:S(2)}, u32[]{:S(2)}) %collective-permute-start.14) | collective-permute-done | bytes 524320 | tf_op jit(solution)/shard_map/ppermute | solution.py:31
  31.1 1.6 %collective-permute-start.4 = (bf16[544,512]{1,0:T(8,128)(2,1)S(1)}, bf16[544,512]{1,0:T(8,128)(2,1)S(1)}, u32[]{:S(2)}, u32[]{:S(2)}) collective-permute-start(bf16[544,512]{1,0:T(8,128)(2,1)S(1)} %get-tuple-element.21), channel_id=1, source_target_pairs={{0,64},{16,80},{32,96},{48,112},{64,128},{80,144},{96,160},{112,17... | collective-permute-start | bytes 1671176 | tf_op jit(solution)/shard_map/ppermute | solution.py:38
  32.7 4.0 %collective-permute-done.18.refs_1_ = bf16[2048,128]{1,0:T(8,128)(2,1)S(1)} collective-permute-done((bf16[2048,128]{1,0:T(8,128)(2,1)S(1)}, bf16[2048,128]{1,0:T(8,128)(2,1)S(1)}, u32[]{:S(2)}, u32[]{:S(2)}) %collective-permute-start.18) | collective-permute-done | bytes 524320 | tf_op jit(solution)/shard_map/ppermute | solution.py:31
  36.7 3.0 %collective-permute-start.5 = (bf16[544,512]{1,0:T(8,128)(2,1)S(1)}, bf16[544,512]{1,0:T(8,128)(2,1)S(1)}, u32[]{:S(2)}, u32[]{:S(2)}) collective-permute-start(bf16[544,512]{1,0:T(8,128)(2,1)S(1)} %get-tuple-element.20), channel_id=1, source_target_pairs={{0,192},{16,208},{32,224},{48,240},{64,0},{80,16},{96,32},{112,48}... | collective-permute-start | bytes 1671176 | tf_op jit(solution)/shard_map/ppermute | solution.py:38
  39.9 2.0 %collective-permute-done.4.refs_4_ = bf16[544,512]{1,0:T(8,128)(2,1)S(1)} collective-permute-done((bf16[544,512]{1,0:T(8,128)(2,1)S(1)}, bf16[544,512]{1,0:T(8,128)(2,1)S(1)}, u32[]{:S(2)}, u32[]{:S(2)}) %collective-permute-start.4) | collective-permute-done | bytes 557088 | tf_op jit(solution)/shard_map/ppermute | solution.py:38
  42.2 4.6 %collective-permute-done.5.refs_5_ = bf16[544,512]{1,0:T(8,128)(2,1)S(1)} collective-permute-done((bf16[544,512]{1,0:T(8,128)(2,1)S(1)}, bf16[544,512]{1,0:T(8,128)(2,1)S(1)}, u32[]{:S(2)}, u32[]{:S(2)}) %collective-permute-start.5) | collective-permute-done | bytes 557088 | tf_op jit(solution)/shard_map/ppermute | solution.py:38
  46.8 3.7 %collective-permute-start.3 = (bf16[544,512]{1,0:T(8,128)(2,1)}, bf16[544,512]{1,0:T(8,128)(2,1)}, u32[]{:S(2)}, u32[]{:S(2)}) collective-permute-start(bf16[544,512]{1,0:T(8,128)(2,1)} %collective-permute-done.2.refs_6_), channel_id=1, source_target_pairs={{0,192},{16,208},{32,224},{48,240},{64,0},{80,16},{96,32},{112,48}... | collective-permute-start | bytes 1671176 | tf_op jit(solution)/shard_map/ppermute | solution.py:38
  51.3 4.4 %collective-permute-done.19.refs_1_ = bf16[2048,128]{1,0:T(8,128)(2,1)S(1)} collective-permute-done((bf16[2048,128]{1,0:T(8,128)(2,1)S(1)}, bf16[2048,128]{1,0:T(8,128)(2,1)S(1)}, u32[]{:S(2)}, u32[]{:S(2)}) %collective-permute-start.19) | collective-permute-done | bytes 524320 | tf_op jit(solution)/shard_map/ppermute | solution.py:31
  62.1 1.2 copy-done.4
  63.3 1.2 copy-done.6
  64.6 1.1 copy-done.8
  65.6 1.1 copy-done.10
  66.7 1.1 copy-done.12
  67.7 1.1 copy-done.14
  68.8 1.1 copy-done.16
  69.8 1.1 copy-done.18
  70.9 2.0 %hold.3 = (bf16[4,1088,512]{2,1,0:T(8,128)(2,1)S(1)}, bf16[4,1088,512]{2,1,0:T(8,128)(2,1)S(1)}) custom-call(s32[1]{0:T(128)S(6)} %select_n.7.refs_0_, s32[1]{0:T(128)S(6)} %select_n.8.refs_1_.refs_0_, bf16[1088,512]{1,0:T(8,128)(2,1)S(1)} %copy-done.4, bf16[544,512]{1,0:T(8,128)(2,1)S(1)} %copy-done.8, bf16[544,512]{1,0:T(8,128)(2,1)S(1)} %copy-done.10, ...), custom_call_target="tpu_custom_call" | custom-call | tf_op jit(solution)/shard_map/hold/pallas_call | solution.py:142
  72.9 1.2 hold.4.refs_1_.refs_2_
  74.1 3.1 %collective-permute-done.20.refs_1_ = bf16[2048,128]{1,0:T(8,128)(2,1)S(1)} collective-permute-done((bf16[2048,128]{1,0:T(8,128)(2,1)S(1)}, bf16[2048,128]{1,0:T(8,128)(2,1)S(1)}, u32[]{:S(2)}, u32[]{:S(2)}) %collective-permute-start.20) | collective-permute-done | bytes 524320 | tf_op jit(solution)/shard_map/ppermute | solution.py:31
  77.2 1.0 shard_map.57.refs_4_
  78.3 1.2 hold.5.refs_2_.refs_3_
  79.5 2.8 %shard_map.58 = (bf16[2048,128]{1,0:T(8,128)(2,1)S(1)}, bf16[2048,128]{1,0:T(8,128)(2,1)S(1)}) custom-call(s32[1]{0:T(128)} %bitcast.core_ref, bf16[2048,128]{1,0:T(8,128)(2,1)S(1)} %collective-permute-done.16.refs_0_, bf16[2048,128]{1,0:T(8,128)(2,1)S(1)} %collective-permute-done.20.refs_1_, bf16[4,1088,512]{2,1,0:T(8,128)(2,1)S(1)} %hold.4.refs_1_.refs_2_, ...), custom_call_target="tpu_custom_call" | custom-call | tf_op jit(solution)/shard_map/pallas_call | solution.py:202
  82.5 2.0 %collective-permute-start.25 = (bf16[2048,128]{1,0:T(8,128)(2,1)S(1)}, bf16[2048,128]{1,0:T(8,128)(2,1)S(1)}, u32[]{:S(2)}, u32[]{:S(2)}) collective-permute-start(bf16[2048,128]{1,0:T(8,128)(2,1)S(1)} %get-tuple-element.28), channel_id=1, source_target_pairs={{0,14},{1,3},{2,0},{3,5},{4,2},{5,7},{6,4},{7,9},{8,6},{9,11},{10,... | collective-permute-start | bytes 1572872 | tf_op jit(solution)/shard_map/ppermute | solution.py:31
  85.6 2.8 %shard_map.60 = (f32[2048,128]{1,0:T(8,128)S(1)}, f32[2048,128]{1,0:T(8,128)S(1)}) custom-call(s32[1]{0:T(128)} %bitcast.core_ref, bf16[2048,128]{1,0:T(8,128)(2,1)S(1)} %collective-permute-done.15.refs_0_, bf16[2048,128]{1,0:T(8,128)(2,1)S(1)} %collective-permute-done.19.refs_1_, bf16[4,1088,512]{2,1,0:T(8,128)(2,1)S(1)} %hold.4.refs_1_.refs_2_, ...), custom_call_target="tpu_custom_call" | custom-call | tf_op jit(solution)/shard_map/pallas_call | solution.py:202
  88.4 3.2 %collective-permute-done.21 = bf16[2048,128]{1,0:T(8,128)(2,1)S(1)} collective-permute-done((bf16[2048,128]{1,0:T(8,128)(2,1)S(1)}, bf16[2048,128]{1,0:T(8,128)(2,1)S(1)}, u32[]{:S(2)}, u32[]{:S(2)}) %collective-permute-start.21) | collective-permute-done | bytes 524320 | tf_op jit(solution)/shard_map/ppermute | solution.py:31
  91.7 1.4 %collective-permute-start.22 = (bf16[2048,128]{1,0:T(8,128)(2,1)S(1)}, bf16[2048,128]{1,0:T(8,128)(2,1)S(1)}, u32[]{:S(2)}, u32[]{:S(2)}) collective-permute-start(bf16[2048,128]{1,0:T(8,128)(2,1)S(1)} %add_convert_fusion.4), channel_id=1, source_target_pairs={{0,14},{1,3},{2,0},{3,5},{4,2},{5,7},{6,4},{7,9},{8,6},{9,11},{10,... | collective-permute-start | bytes 1572872 | tf_op jit(solution)/shard_map/ppermute | solution.py:31
  93.1 4.1 %collective-permute-done.25 = bf16[2048,128]{1,0:T(8,128)(2,1)S(1)} collective-permute-done((bf16[2048,128]{1,0:T(8,128)(2,1)S(1)}, bf16[2048,128]{1,0:T(8,128)(2,1)S(1)}, u32[]{:S(2)}, u32[]{:S(2)}) %collective-permute-start.25) | collective-permute-done | bytes 524320 | tf_op jit(solution)/shard_map/ppermute | solution.py:31
  97.3 1.6 %collective-permute-start.26 = (bf16[2048,128]{1,0:T(8,128)(2,1)S(1)}, bf16[2048,128]{1,0:T(8,128)(2,1)S(1)}, u32[]{:S(2)}, u32[]{:S(2)}) collective-permute-start(bf16[2048,128]{1,0:T(8,128)(2,1)S(1)} %add_convert_fusion.1), channel_id=1, source_target_pairs={{0,14},{1,3},{2,0},{3,5},{4,2},{5,7},{6,4},{7,9},{8,6},{9,11},{10,... | collective-permute-start | bytes 1572872 | tf_op jit(solution)/shard_map/ppermute | solution.py:31
  99.0 1.0 shard_map.61.refs_4_
  100.0 2.8 %shard_map.62 = (f32[2048,128]{1,0:T(8,128)S(1)}, f32[2048,128]{1,0:T(8,128)S(1)}) custom-call(s32[1]{0:T(128)} %bitcast.core_ref, bf16[2048,128]{1,0:T(8,128)(2,1)S(1)} %collective-permute-done.14.refs_0_, bf16[2048,128]{1,0:T(8,128)(2,1)S(1)} %collective-permute-done.18.refs_1_, bf16[4,1088,512]{2,1,0:T(8,128)(2,1)S(1)} %hold.4.refs_1_.refs_2_, ...), custom_call_target="tpu_custom_call" | custom-call | tf_op jit(solution)/shard_map/pallas_call | solution.py:202
  102.9 1.4 %collective-permute-start.23 = (bf16[2048,128]{1,0:T(8,128)(2,1)S(1)}, bf16[2048,128]{1,0:T(8,128)(2,1)S(1)}, u32[]{:S(2)}, u32[]{:S(2)}) collective-permute-start(bf16[2048,128]{1,0:T(8,128)(2,1)S(1)} %add_convert_fusion.3), channel_id=1, source_target_pairs={{0,14},{1,3},{2,0},{3,5},{4,2},{5,7},{6,4},{7,9},{8,6},{9,11},{10,... | collective-permute-start | bytes 1572872 | tf_op jit(solution)/shard_map/ppermute | solution.py:31
  104.4 4.1 %collective-permute-done.26 = bf16[2048,128]{1,0:T(8,128)(2,1)S(1)} collective-permute-done((bf16[2048,128]{1,0:T(8,128)(2,1)S(1)}, bf16[2048,128]{1,0:T(8,128)(2,1)S(1)}, u32[]{:S(2)}, u32[]{:S(2)}) %collective-permute-start.26) | collective-permute-done | bytes 524320 | tf_op jit(solution)/shard_map/ppermute | solution.py:31
  108.6 1.4 %collective-permute-start.27 = (bf16[2048,128]{1,0:T(8,128)(2,1)S(1)}, bf16[2048,128]{1,0:T(8,128)(2,1)S(1)}, u32[]{:S(2)}, u32[]{:S(2)}) collective-permute-start(bf16[2048,128]{1,0:T(8,128)(2,1)S(1)} %add_convert_fusion), channel_id=1, source_target_pairs={{0,14},{1,3},{2,0},{3,5},{4,2},{5,7},{6,4},{7,9},{8,6},{9,11},{10,... | collective-permute-start | bytes 1572872 | tf_op jit(solution)/shard_map/ppermute | solution.py:31
  110.9 2.4 %shard_map.64 = f32[2048,128]{1,0:T(8,128)S(1)} custom-call(s32[1]{0:T(128)} %bitcast.core_ref, bf16[2048,128]{1,0:T(8,128)(2,1)S(1)} %copy-done.2, bf16[4,1088,512]{2,1,0:T(8,128)(2,1)S(1)} %hold.4.refs_1_.refs_2_, bf16[4,1088,512]{2,1,0:T(8,128)(2,1)S(1)} %hold.5.refs_2_.refs_3_, bf16[352,128]{1,0:T(8,128)(2,1)S(1)} %shard_map.63.refs_3_), custom_call_target="tpu_custom_call" | custom-call | tf_op jit(solution)/shard_map/pallas_call | solution.py:202
  114.2 1.4 %collective-permute-start.24 = (bf16[2048,128]{1,0:T(8,128)(2,1)S(1)}, bf16[2048,128]{1,0:T(8,128)(2,1)S(1)}, u32[]{:S(2)}, u32[]{:S(2)}) collective-permute-start(bf16[2048,128]{1,0:T(8,128)(2,1)S(1)} %add_convert_fusion.2), channel_id=1, source_target_pairs={{0,14},{1,3},{2,0},{3,5},{4,2},{5,7},{6,4},{7,9},{8,6},{9,11},{10,... | collective-permute-start | bytes 1572872 | tf_op jit(solution)/shard_map/ppermute | solution.py:31
  115.6 4.1 %collective-permute-done.27 = bf16[2048,128]{1,0:T(8,128)(2,1)S(1)} collective-permute-done((bf16[2048,128]{1,0:T(8,128)(2,1)S(1)}, bf16[2048,128]{1,0:T(8,128)(2,1)S(1)}, u32[]{:S(2)}, u32[]{:S(2)}) %collective-permute-start.27) | collective-permute-done | bytes 524320 | tf_op jit(solution)/shard_map/ppermute | solution.py:31
  120.6 2.4 %shard_map.56.own = f32[2048,128]{1,0:T(8,128)S(1)} custom-call(s32[1]{0:T(128)} %bitcast.core_ref, bf16[2048,128]{1,0:T(8,128)(2,1)S(1)} %copy-done, bf16[4,1088,512]{2,1,0:T(8,128)(2,1)S(1)} %hold.4.refs_1_.refs_2_, bf16[4,1088,512]{2,1,0:T(8,128)(2,1)S(1)} %hold.5.refs_2_.refs_3_, bf16[352,128]{1,0:T(8,128)(2,1)S(1)} %shard_map.55.refs_3_), custom_call_target="tpu_custom_call" | custom-call | tf_op jit(solution)/shard_map/pallas_call | solution.py:202
  123.1 2.2 %collective-permute-done.24.first = bf16[2048,128]{1,0:T(8,128)(2,1)S(1)} collective-permute-done((bf16[2048,128]{1,0:T(8,128)(2,1)S(1)}, bf16[2048,128]{1,0:T(8,128)(2,1)S(1)}, u32[]{:S(2)}, u32[]{:S(2)}) %collective-permute-start.24) | collective-permute-done | bytes 524320 | tf_op jit(solution)/shard_map/ppermute | solution.py:31
  125.3 1.0 close.1
  (71 shorter events, 12.3 us)
Async XLA Ops:
  2.7 18.1 %all-to-all-start = ((bf16[4,1088,128]{2,1,0:T(8,128)(2,1)}), bf16[4,1088,128]{2,1,0:T(8,128)(2,1)S(1)}, u32[]{:S(2)}, u32[]{:S(2)}) async-start(bf16[4,1088,128]{2,1,0:T(8,128)(2,1)} %get-tuple-element.19), calls=%async_computation | async-start | bytes 2228224 | tf_op jit(solution)/shard_map/all_to_all | solution.py:46
  8.4 12.3 %collective-permute-start.13 = (bf16[2048,128]{1,0:T(8,128)(2,1)}, bf16[2048,128]{1,0:T(8,128)(2,1)S(1)}, u32[]{:S(2)}, u32[]{:S(2)}) collective-permute-start(bf16[2048,128]{1,0:T(8,128)(2,1)} %get-tuple-element.18.refs_0_), channel_id=1, source_target_pairs={{0,2},{1,15},{2,4},{3,1},{4,6},{5,3},{6,8},{7,5},{8,10},{9,7},{10,... | collective-permute-start | bytes 1572872 | tf_op jit(solution)/shard_map/ppermute | solution.py:31
  9.4 13.9 %collective-permute-start.17 = (bf16[2048,128]{1,0:T(8,128)(2,1)}, bf16[2048,128]{1,0:T(8,128)(2,1)S(1)}, u32[]{:S(2)}, u32[]{:S(2)}) collective-permute-start(bf16[2048,128]{1,0:T(8,128)(2,1)} %get-tuple-element.18.refs_0_), channel_id=1, source_target_pairs={{0,1},{1,0},{2,3},{3,2},{4,5},{5,4},{6,7},{7,6},{8,9},{9,8},{10,11... | collective-permute-start | bytes 1572872 | tf_op jit(solution)/shard_map/ppermute | solution.py:42
  20.7 19.0 %copy-start.1 = (bf16[2048,128]{1,0:T(8,128)(2,1)}, bf16[2048,128]{1,0:T(8,128)(2,1)S(1)}, u32[]{:S(2)}) copy-start(bf16[2048,128]{1,0:T(8,128)(2,1)S(1)} %collective-permute-done.13.refs_0_) | copy-start | bytes 1572868
  20.7 10.4 %collective-permute-start.14 = (bf16[2048,128]{1,0:T(8,128)(2,1)S(1)}, bf16[2048,128]{1,0:T(8,128)(2,1)S(1)}, u32[]{:S(2)}, u32[]{:S(2)}) collective-permute-start(bf16[2048,128]{1,0:T(8,128)(2,1)S(1)} %collective-permute-done.13.refs_0_), channel_id=1, source_target_pairs={{0,2},{1,15},{2,4},{3,1},{4,6},{5,3},{6,8},{7,5},{8,10},{9,7},{10,... | collective-permute-start | bytes 1572872 | tf_op jit(solution)/shard_map/ppermute | solution.py:31
  21.0 35.5 %collective-permute-start.6 = (bf16[1088,512]{1,0:T(8,128)(2,1)S(1)}, bf16[1088,512]{1,0:T(8,128)(2,1)S(1)}, u32[]{:S(2)}, u32[]{:S(2)}) collective-permute-start(bf16[1088,512]{1,0:T(8,128)(2,1)S(1)} %get-tuple-element.22.refs_2_), channel_id=1, source_target_pairs={{0,1},{1,0},{2,3},{3,2},{4,5},{5,4},{6,7},{7,6},{8,9},{9,8},{10,11... | collective-permute-start | bytes 3342344 | tf_op jit(solution)/shard_map/ppermute | solution.py:42
  22.2 1.0 copy-start.3
  23.3 13.4 %collective-permute-start.18 = (bf16[2048,128]{1,0:T(8,128)(2,1)S(1)}, bf16[2048,128]{1,0:T(8,128)(2,1)S(1)}, u32[]{:S(2)}, u32[]{:S(2)}) collective-permute-start(bf16[2048,128]{1,0:T(8,128)(2,1)S(1)} %collective-permute-done.17), channel_id=1, source_target_pairs={{0,2},{1,15},{2,4},{3,1},{4,6},{5,3},{6,8},{7,5},{8,10},{9,7},{10,... | collective-permute-start | bytes 1572872 | tf_op jit(solution)/shard_map/ppermute | solution.py:31
  23.3 16.5 %collective-permute-start = (bf16[544,512]{1,0:T(8,128)(2,1)S(1)}, bf16[544,512]{1,0:T(8,128)(2,1)S(1)}, u32[]{:S(2)}, u32[]{:S(2)}) collective-permute-start(bf16[544,512]{1,0:T(8,128)(2,1)S(1)} %get-tuple-element.20), channel_id=1, source_target_pairs={{0,64},{16,80},{32,96},{48,112},{64,128},{80,144},{96,160},{112,17... | collective-permute-start | bytes 1671176 | tf_op jit(solution)/shard_map/ppermute | solution.py:38
  25.0 14.7 %collective-permute-start.2 = (bf16[544,512]{1,0:T(8,128)(2,1)S(1)}, bf16[544,512]{1,0:T(8,128)(2,1)}, u32[]{:S(2)}, u32[]{:S(2)}) collective-permute-start(bf16[544,512]{1,0:T(8,128)(2,1)S(1)} %get-tuple-element.21), channel_id=1, source_target_pairs={{0,192},{16,208},{32,224},{48,240},{64,0},{80,16},{96,32},{112,48}... | collective-permute-start | bytes 1671176 | tf_op jit(solution)/shard_map/ppermute | solution.py:38
  31.1 10.7 %collective-permute-start.4 = (bf16[544,512]{1,0:T(8,128)(2,1)S(1)}, bf16[544,512]{1,0:T(8,128)(2,1)S(1)}, u32[]{:S(2)}, u32[]{:S(2)}) collective-permute-start(bf16[544,512]{1,0:T(8,128)(2,1)S(1)} %get-tuple-element.21), channel_id=1, source_target_pairs={{0,64},{16,80},{32,96},{48,112},{64,128},{80,144},{96,160},{112,17... | collective-permute-start | bytes 1671176 | tf_op jit(solution)/shard_map/ppermute | solution.py:38
  36.7 10.1 %collective-permute-start.5 = (bf16[544,512]{1,0:T(8,128)(2,1)S(1)}, bf16[544,512]{1,0:T(8,128)(2,1)S(1)}, u32[]{:S(2)}, u32[]{:S(2)}) collective-permute-start(bf16[544,512]{1,0:T(8,128)(2,1)S(1)} %get-tuple-element.20), channel_id=1, source_target_pairs={{0,192},{16,208},{32,224},{48,240},{64,0},{80,16},{96,32},{112,48}... | collective-permute-start | bytes 1671176 | tf_op jit(solution)/shard_map/ppermute | solution.py:38
  39.7 10.7 %collective-permute-start.15 = (bf16[2048,128]{1,0:T(8,128)(2,1)S(1)}, bf16[2048,128]{1,0:T(8,128)(2,1)S(1)}, u32[]{:S(2)}, u32[]{:S(2)}) collective-permute-start(bf16[2048,128]{1,0:T(8,128)(2,1)S(1)} %collective-permute-done.14.refs_0_), channel_id=1, source_target_pairs={{0,2},{1,15},{2,4},{3,1},{4,6},{5,3},{6,8},{7,5},{8,10},{9,7},{10,... | collective-permute-start | bytes 1572872 | tf_op jit(solution)/shard_map/ppermute | solution.py:31
  39.8 16.0 %collective-permute-start.19 = (bf16[2048,128]{1,0:T(8,128)(2,1)S(1)}, bf16[2048,128]{1,0:T(8,128)(2,1)S(1)}, u32[]{:S(2)}, u32[]{:S(2)}) collective-permute-start(bf16[2048,128]{1,0:T(8,128)(2,1)S(1)} %collective-permute-done.18.refs_1_), channel_id=1, source_target_pairs={{0,2},{1,15},{2,4},{3,1},{4,6},{5,3},{6,8},{7,5},{8,10},{9,7},{10,... | collective-permute-start | bytes 1572872 | tf_op jit(solution)/shard_map/ppermute | solution.py:31
  41.9 17.0 %collective-permute-start.1 = (bf16[544,512]{1,0:T(8,128)(2,1)S(1)}, bf16[544,512]{1,0:T(8,128)(2,1)}, u32[]{:S(2)}, u32[]{:S(2)}) collective-permute-start(bf16[544,512]{1,0:T(8,128)(2,1)S(1)} %collective-permute-done.refs_3_), channel_id=1, source_target_pairs={{0,64},{16,80},{32,96},{48,112},{64,128},{80,144},{96,160},{112,17... | collective-permute-start | bytes 1671176 | tf_op jit(solution)/shard_map/ppermute | solution.py:38
  46.8 12.1 %collective-permute-start.3 = (bf16[544,512]{1,0:T(8,128)(2,1)}, bf16[544,512]{1,0:T(8,128)(2,1)}, u32[]{:S(2)}, u32[]{:S(2)}) collective-permute-start(bf16[544,512]{1,0:T(8,128)(2,1)} %collective-permute-done.2.refs_6_), channel_id=1, source_target_pairs={{0,192},{16,208},{32,224},{48,240},{64,0},{80,16},{96,32},{112,48}... | collective-permute-start | bytes 1671176 | tf_op jit(solution)/shard_map/ppermute | solution.py:38
  50.5 8.9 %collective-permute-start.7 = (bf16[544,512]{1,0:T(8,128)(2,1)S(1)}, bf16[544,512]{1,0:T(8,128)(2,1)S(1)}, u32[]{:S(2)}, u32[]{:S(2)}) collective-permute-start(bf16[544,512]{1,0:T(8,128)(2,1)S(1)} %collective-permute-done.refs_3_), channel_id=1, source_target_pairs={{0,1},{1,0},{2,3},{3,2},{4,5},{5,4},{6,7},{7,6},{8,9},{9,8},{10,11... | collective-permute-start | bytes 1671176 | tf_op jit(solution)/shard_map/ppermute | solution.py:42
  50.5 0.8 copy-start.7
  55.8 4.6 %collective-permute-start.8 = (bf16[544,512]{1,0:T(8,128)(2,1)S(1)}, bf16[544,512]{1,0:T(8,128)(2,1)S(1)}, u32[]{:S(2)}, u32[]{:S(2)}) collective-permute-start(bf16[544,512]{1,0:T(8,128)(2,1)S(1)} %collective-permute-done.4.refs_4_), channel_id=1, source_target_pairs={{0,1},{1,0},{2,3},{3,2},{4,5},{5,4},{6,7},{7,6},{8,9},{9,8},{10,11... | collective-permute-start | bytes 1671176 | tf_op jit(solution)/shard_map/ppermute | solution.py:42
  56.6 1.0 copy-start.5
  57.6 3.6 %collective-permute-start.9 = (bf16[544,512]{1,0:T(8,128)(2,1)S(1)}, bf16[544,512]{1,0:T(8,128)(2,1)S(1)}, u32[]{:S(2)}, u32[]{:S(2)}) collective-permute-start(bf16[544,512]{1,0:T(8,128)(2,1)S(1)} %collective-permute-done.5.refs_5_), channel_id=1, source_target_pairs={{0,1},{1,0},{2,3},{3,2},{4,5},{5,4},{6,7},{7,6},{8,9},{9,8},{10,11... | collective-permute-start | bytes 1671176 | tf_op jit(solution)/shard_map/ppermute | solution.py:42
  58.1 0.8 copy-start.11
  58.9 3.2 %collective-permute-start.10 = (bf16[544,512]{1,0:T(8,128)(2,1)}, bf16[544,512]{1,0:T(8,128)(2,1)}, u32[]{:S(2)}, u32[]{:S(2)}) collective-permute-start(bf16[544,512]{1,0:T(8,128)(2,1)} %collective-permute-done.2.refs_6_), channel_id=1, source_target_pairs={{0,1},{1,0},{2,3},{3,2},{4,5},{5,4},{6,7},{7,6},{8,9},{9,8},{10,11... | collective-permute-start | bytes 1671176 | tf_op jit(solution)/shard_map/ppermute | solution.py:42
  58.9 19.3 %collective-permute-start.11 = (bf16[544,512]{1,0:T(8,128)(2,1)}, bf16[544,512]{1,0:T(8,128)(2,1)}, u32[]{:S(2)}, u32[]{:S(2)}) collective-permute-start(bf16[544,512]{1,0:T(8,128)(2,1)} %collective-permute-done.1.refs_1_), channel_id=1, source_target_pairs={{0,1},{1,0},{2,3},{3,2},{4,5},{5,4},{6,7},{7,6},{8,9},{9,8},{10,11... | collective-permute-start | bytes 1671176 | tf_op jit(solution)/shard_map/ppermute | solution.py:42
  59.4 0.9 copy-start.13
  60.3 18.0 %collective-permute-start.12 = (bf16[544,512]{1,0:T(8,128)(2,1)}, bf16[544,512]{1,0:T(8,128)(2,1)}, u32[]{:S(2)}, u32[]{:S(2)}) collective-permute-start(bf16[544,512]{1,0:T(8,128)(2,1)} %collective-permute-done.3.refs_2_), channel_id=1, source_target_pairs={{0,1},{1,0},{2,3},{3,2},{4,5},{5,4},{6,7},{7,6},{8,9},{9,8},{10,11... | collective-permute-start | bytes 1671176 | tf_op jit(solution)/shard_map/ppermute | solution.py:42
  60.4 0.9 copy-start.15
  61.2 12.9 %collective-permute-start.16 = (bf16[2048,128]{1,0:T(8,128)(2,1)S(1)}, bf16[2048,128]{1,0:T(8,128)(2,1)S(1)}, u32[]{:S(2)}, u32[]{:S(2)}) collective-permute-start(bf16[2048,128]{1,0:T(8,128)(2,1)S(1)} %collective-permute-done.15.refs_0_), channel_id=1, source_target_pairs={{0,2},{1,15},{2,4},{3,1},{4,6},{5,3},{6,8},{7,5},{8,10},{9,7},{10,... | collective-permute-start | bytes 1572872 | tf_op jit(solution)/shard_map/ppermute | solution.py:31
  61.2 0.8 copy-start.17
  62.0 15.2 %collective-permute-start.20 = (bf16[2048,128]{1,0:T(8,128)(2,1)S(1)}, bf16[2048,128]{1,0:T(8,128)(2,1)S(1)}, u32[]{:S(2)}, u32[]{:S(2)}) collective-permute-start(bf16[2048,128]{1,0:T(8,128)(2,1)S(1)} %collective-permute-done.19.refs_1_), channel_id=1, source_target_pairs={{0,2},{1,15},{2,4},{3,1},{4,6},{5,3},{6,8},{7,5},{8,10},{9,7},{10,... | collective-permute-start | bytes 1572872 | tf_op jit(solution)/shard_map/ppermute | solution.py:31
  62.1 1.2 copy-start.4
  63.3 1.2 copy-start.6
  64.5 1.1 copy-start.8
  65.6 1.1 copy-start.10
  66.7 1.1 copy-start.12
  67.7 1.1 copy-start.14
  68.8 1.1 copy-start.16
  69.8 1.1 copy-start.18
  82.3 9.3 %collective-permute-start.21 = (bf16[2048,128]{1,0:T(8,128)(2,1)S(1)}, bf16[2048,128]{1,0:T(8,128)(2,1)S(1)}, u32[]{:S(2)}, u32[]{:S(2)}) collective-permute-start(bf16[2048,128]{1,0:T(8,128)(2,1)S(1)} %get-tuple-element.25), channel_id=1, source_target_pairs={{0,14},{1,3},{2,0},{3,5},{4,2},{5,7},{6,4},{7,9},{8,6},{9,11},{10,... | collective-permute-start | bytes 1572872 | tf_op jit(solution)/shard_map/ppermute | solution.py:31
  82.5 14.7 %collective-permute-start.25 = (bf16[2048,128]{1,0:T(8,128)(2,1)S(1)}, bf16[2048,128]{1,0:T(8,128)(2,1)S(1)}, u32[]{:S(2)}, u32[]{:S(2)}) collective-permute-start(bf16[2048,128]{1,0:T(8,128)(2,1)S(1)} %get-tuple-element.28), channel_id=1, source_target_pairs={{0,14},{1,3},{2,0},{3,5},{4,2},{5,7},{6,4},{7,9},{8,6},{9,11},{10,... | collective-permute-start | bytes 1572872 | tf_op jit(solution)/shard_map/ppermute | solution.py:31
  91.7 11.1 %collective-permute-start.22 = (bf16[2048,128]{1,0:T(8,128)(2,1)S(1)}, bf16[2048,128]{1,0:T(8,128)(2,1)S(1)}, u32[]{:S(2)}, u32[]{:S(2)}) collective-permute-start(bf16[2048,128]{1,0:T(8,128)(2,1)S(1)} %add_convert_fusion.4), channel_id=1, source_target_pairs={{0,14},{1,3},{2,0},{3,5},{4,2},{5,7},{6,4},{7,9},{8,6},{9,11},{10,... | collective-permute-start | bytes 1572872 | tf_op jit(solution)/shard_map/ppermute | solution.py:31
  97.3 11.1 %collective-permute-start.26 = (bf16[2048,128]{1,0:T(8,128)(2,1)S(1)}, bf16[2048,128]{1,0:T(8,128)(2,1)S(1)}, u32[]{:S(2)}, u32[]{:S(2)}) collective-permute-start(bf16[2048,128]{1,0:T(8,128)(2,1)S(1)} %add_convert_fusion.1), channel_id=1, source_target_pairs={{0,14},{1,3},{2,0},{3,5},{4,2},{5,7},{6,4},{7,9},{8,6},{9,11},{10,... | collective-permute-start | bytes 1572872 | tf_op jit(solution)/shard_map/ppermute | solution.py:31
  102.8 7.2 %copy-start.2 = (bf16[2048,128]{1,0:T(8,128)(2,1)S(1)}, bf16[2048,128]{1,0:T(8,128)(2,1)}, u32[]{:S(2)}) copy-start(bf16[2048,128]{1,0:T(8,128)(2,1)} %copy-done.1) | copy-start | bytes 1572868
  102.9 11.1 %collective-permute-start.23 = (bf16[2048,128]{1,0:T(8,128)(2,1)S(1)}, bf16[2048,128]{1,0:T(8,128)(2,1)S(1)}, u32[]{:S(2)}, u32[]{:S(2)}) collective-permute-start(bf16[2048,128]{1,0:T(8,128)(2,1)S(1)} %add_convert_fusion.3), channel_id=1, source_target_pairs={{0,14},{1,3},{2,0},{3,5},{4,2},{5,7},{6,4},{7,9},{8,6},{9,11},{10,... | collective-permute-start | bytes 1572872 | tf_op jit(solution)/shard_map/ppermute | solution.py:31
  108.6 11.1 %collective-permute-start.27 = (bf16[2048,128]{1,0:T(8,128)(2,1)S(1)}, bf16[2048,128]{1,0:T(8,128)(2,1)S(1)}, u32[]{:S(2)}, u32[]{:S(2)}) collective-permute-start(bf16[2048,128]{1,0:T(8,128)(2,1)S(1)} %add_convert_fusion), channel_id=1, source_target_pairs={{0,14},{1,3},{2,0},{3,5},{4,2},{5,7},{6,4},{7,9},{8,6},{9,11},{10,... | collective-permute-start | bytes 1572872 | tf_op jit(solution)/shard_map/ppermute | solution.py:31
  110.9 8.8 %copy-start = (bf16[2048,128]{1,0:T(8,128)(2,1)S(1)}, bf16[2048,128]{1,0:T(8,128)(2,1)}, u32[]{:S(2)}) copy-start(bf16[2048,128]{1,0:T(8,128)(2,1)} %get-tuple-element.18.refs_0_) | copy-start | bytes 1572868
  114.2 11.1 %collective-permute-start.24 = (bf16[2048,128]{1,0:T(8,128)(2,1)S(1)}, bf16[2048,128]{1,0:T(8,128)(2,1)S(1)}, u32[]{:S(2)}, u32[]{:S(2)}) collective-permute-start(bf16[2048,128]{1,0:T(8,128)(2,1)S(1)} %add_convert_fusion.2), channel_id=1, source_target_pairs={{0,14},{1,3},{2,0},{3,5},{4,2},{5,7},{6,4},{7,9},{8,6},{9,11},{10,... | collective-permute-start | bytes 1572872 | tf_op jit(solution)/shard_map/ppermute | solution.py:31
  119.7 5.6 %collective-permute-start.28 = (bf16[2048,128]{1,0:T(8,128)(2,1)S(1)}, bf16[2048,128]{1,0:T(8,128)(2,1)S(1)}, u32[]{:S(2)}, u32[]{:S(2)}) collective-permute-start(bf16[2048,128]{1,0:T(8,128)(2,1)S(1)} %collective-permute-done.27), channel_id=1, source_target_pairs={{0,1},{1,0},{2,3},{3,2},{4,5},{5,4},{6,7},{7,6},{8,9},{9,8},{10,11... | collective-permute-start | bytes 1572872 | tf_op jit(solution)/shard_map/ppermute | solution.py:42
  (1 other events, 0.8 us)
where the time goes:
time: 127 us; the launch traced here: 126 us
  waiting for transfers between devices  49.7 us (39%)
  starting transfers between devices  33.5 us (26%)
  Pallas kernels  26.6 us (21%)
  local copies, waits for them, and re-layouts  15.8 us (12%)
    ppermute x14, waiting for transfers between devices, onward(): return lax.ppermute(x, ('z', 'c'), pairs)  43.1 us
    pallas_call x10, Pallas kernels, call(): pl.pallas_call(functools.partial(body, n, units), out_shape=out_shape, in...  18.1 us
    unnamed x38, local copies, waits for them, and re-layouts  15.8 us
    ppermute x6, starting transfers between devices, along_column(): return lax.ppermute(x, ('y', 'x', 'c'), pairs)  11.9 us
    ppermute x14, starting transfers between devices, onward(): return lax.ppermute(x, ('z', 'c'), pairs)  10.6 us
    ppermute x6, waiting for transfers between devices, along_column(): return lax.ppermute(x, ('y', 'x', 'c'), pairs)  6.58 us
    all_to_all x1, starting transfers between devices, from_four(): lax.all_to_all(copies, AXES, 0, 0, axis_index_groups=groups, tiled=True)  5.74 us
    ppermute x9, starting transfers between devices, swap(): return lax.ppermute(x, 'c', [(0, 1), (1, 0)])  5.18 us
  transfers between devices with their start and end apart: 30, of which 13 were waited for; matrix products, arithmetic and copies ran while one was open for 0% of the time, Pallas kernels for 15%

commit v1 on v0

--- a/solution.py
+++ b/solution.py
@@ -120,35 +120,33 @@
 PARTS = ((0, None), (3, 0), (3, 1), (1, 0), (1, 1), (2, 0), (2, 1))
 
 
-def hold_body(parts, sides, *refs):
-    n, places, refs = len(parts), refs[:sides], refs[sides:]
-    outs, sems = refs[-1 - sides : -1], refs[-1]
-    half, copies = outs[0].shape[1] // 2, []
-    for s, out in enumerate(outs):
-        for i, (by, h) in enumerate(parts):
-            at = (places[s][0] + by) % 4
-            end = out.at[at] if h is None else out.at[at, half * h : half * (h + 1)]
-            copies.append(pltpu.make_async_copy(refs[n * s + i], end, sems.at[n * s + i]))
+def hold_body(parts, place_ref, *refs):
+    n = len(parts)
+    blocks, out, sems = refs[:n], refs[-2], refs[-1]
+    half, at = out.shape[1] // 2, place_ref[0]
+    copies = []
+    for i, (by, h) in enumerate(parts):
+        end = out.at[(at + by) % 4] if h is None else out.at[(at + by) % 4, half * h : half * (h + 1)]
+        copies.append(pltpu.make_async_copy(blocks[i], end, sems.at[i]))
     for c in copies:
         c.start()
     for c in copies:
         c.wait()
 
 
-def hold(places, parts, blocks, shape, so_far=None):
-    n, sides = len(blocks), len(places)
+def hold(place, parts, blocks, shape, so_far=None):
+    n = len(parts)
     more = [] if so_far is None else [so_far]
-    remote = pl.BlockSpec(memory_space=pltpu.HBM)
-    return pl.pallas_call(
-        functools.partial(hold_body, parts, sides),
-        out_shape=[jax.ShapeDtypeStruct(shape, bf16)] * sides,
-        in_specs=[pl.BlockSpec(memory_space=pltpu.SMEM)] * sides + [remote] * n + [WHOLE] * len(more),
-        out_specs=[WHOLE] * sides,
-        input_output_aliases={n + sides: 0} if more else {},
+    return pl.pallas_call(
+        functools.partial(hold_body, parts),
+        out_shape=jax.ShapeDtypeStruct(shape, bf16),
+        in_specs=[pl.BlockSpec(memory_space=pltpu.SMEM)] + [pl.BlockSpec(memory_space=pltpu.HBM)] * n + [WHOLE] * len(more),
+        out_specs=WHOLE,
+        input_output_aliases={n + 1: 0} if more else {},
         scratch_shapes=[pltpu.SemaphoreType.DMA((n,))],
         compiler_params=SMALL,
         name="hold",
-    )(*places, *blocks, *more)
+    )(place, *blocks, *more)
 
 
 def order(core, b, w):
@@ -258,12 +256,14 @@
         others.append(swap(b))
     row, column = lax.axis_index("y").astype(jnp.int32)[None], lax.axis_index("x").astype(jnp.int32)[None]
     first = core == 0
-    mine, other = jnp.where(first, row, column), jnp.where(first, column, row)
     shape = (4, *here.shape)
-    columns, others_columns = hold([mine, other], PARTS[:5], [*blocks[:5], *others[:5]], shape)
-    (columns,) = hold([mine], PARTS[5:], blocks[5:], shape, columns)
-    (others_columns,) = hold([other], PARTS[5:], others[5:], shape, others_columns)
-    weights = columns, others_columns
+
+    def held(place, blocks):
+        most = hold(place, PARTS[:5], blocks[:5], shape)
+        return hold(place, PARTS[5:], blocks[5:], shape, most)
+
+    columns = held(jnp.where(first, row, column), blocks)
+    weights = columns, held(jnp.where(first, column, row), others)
 
     units = down_weight.shape[0]
     groups = [(own[4], mate[3]), (own[3], mate[2]), (own[2], mate[1]), (own[1],), (own[0],)]

time: 127 us -> 127 us (level)
  waiting for transfers between devices: 49.7 us -> 55 us
  local copies, waits for them, and re-layouts: 15.8 us -> 12 us
  starting transfers between devices: 33.5 us -> 30.8 us
    ppermute x14, waiting for transfers between devices: 43.1 us -> 48.4 us  [onward(): return lax.ppermute(x, ('z', 'c'), pairs)]
    unnamed x38, local copies, waits for them, and re-layouts: 15.8 us -> 12 us
    ppermute x14, starting transfers between devices: 10.6 us -> 7.96 us  [onward(): return lax.ppermute(x, ('z', 'c'), pairs)]
    pallas_call x3 -> x4, Pallas kernels: 4.47 us -> 5.61 us  [hold(): pl.pallas_call(functools.partial(hold_body, parts), out_shape=jax.ShapeDt...]
  transfers between devices with their start and end apart: 30 -> 30, of which waited for: 13 -> 15; matrix products, arithmetic and copies ran while one was open for 0% -> 0% of each run, Pallas kernels for 15% -> 16%
where the time goes in v1:
time: 127 us; the launch traced here: 126 us
  waiting for transfers between devices  55 us (43%)
  starting transfers between devices  30.8 us (24%)
  Pallas kernels  27.7 us (22%)
  local copies, waits for them, and re-layouts  12 us (9%)
    ppermute x14, waiting for transfers between devices, onward(): return lax.ppermute(x, ('z', 'c'), pairs)  48.4 us
    pallas_call x10, Pallas kernels, call(): pl.pallas_call(functools.partial(body, n, units), out_shape=out_shape, in...  18.1 us
    unnamed x38, local copies, waits for them, and re-layouts  12 us
    ppermute x6, starting transfers between devices, along_column(): return lax.ppermute(x, ('y', 'x', 'c'), pairs)  11.9 us
    ppermute x14, starting transfers between devices, onward(): return lax.ppermute(x, ('z', 'c'), pairs)  7.96 us
    ppermute x6, waiting for transfers between devices, along_column(): return lax.ppermute(x, ('y', 'x', 'c'), pairs)  6.58 us
    all_to_all x1, starting transfers between devices, from_four(): lax.all_to_all(copies, AXES, 0, 0, axis_index_groups=groups, tiled=True)  5.74 us
    pallas_call x4, Pallas kernels, hold(): pl.pallas_call(functools.partial(hold_body, parts), out_shape=jax.ShapeDt...  5.61 us
  transfers between devices with their start and end apart: 30, of which 15 were waited for; matrix products, arithmetic and copies ran while one was open for 0% of the time, Pallas kernels for 16%

profile of v1, /device:TPU:2, one launch (start us, length us, event | category | flops | bytes accessed | tf_op | source)
XLA Modules:
  0.0 126.3 jit_solution(16584072202833144023)
XLA Ops:
  0.0 2.7 %opening.1 = (bf16[2048,128]{1,0:T(8,128)(2,1)}, bf16[4,1088,128]{2,1,0:T(8,128)(2,1)}) custom-call(bf16[128,2048]{1,0:T(8,128)(2,1)} %tokens_in.1, f32[1,2048]{1,0:T(1,128)} %bitcast.8, bf16[352,128]{1,0:T(8,128)(2,1)} %bitcast.6, bf16[352,128]{1,0:T(8,128)(2,1)} %bitcast.7, bf16[352,128]{1,0:T(8,128)(2,1)} %down_in.1), custom_call_target="tpu_custom_call" | custom-call | tf_op jit(solution)/shard_map/opening/pallas_call | solution.py:82
  2.7 5.7 %all-to-all-start = ((bf16[4,1088,128]{2,1,0:T(8,128)(2,1)}), bf16[4,1088,128]{2,1,0:T(8,128)(2,1)S(1)}, u32[]{:S(2)}, u32[]{:S(2)}) async-start(bf16[4,1088,128]{2,1,0:T(8,128)(2,1)} %get-tuple-element.17), calls=%async_computation | async-start | bytes 2228224 | tf_op jit(solution)/shard_map/all_to_all | solution.py:46
  8.4 1.0 collective-permute-start.13
  9.4 2.9 %collective-permute-start.17 = (bf16[2048,128]{1,0:T(8,128)(2,1)}, bf16[2048,128]{1,0:T(8,128)(2,1)S(1)}, u32[]{:S(2)}, u32[]{:S(2)}) collective-permute-start(bf16[2048,128]{1,0:T(8,128)(2,1)} %get-tuple-element.16.refs_0_), channel_id=1, source_target_pairs={{0,1},{1,0},{2,3},{3,2},{4,5},{5,4},{6,7},{7,6},{8,9},{9,8},{10,11... | collective-permute-start | bytes 1572872 | tf_op jit(solution)/shard_map/ppermute | solution.py:42
  12.3 8.5 %collective-permute-done.13.refs_0_ = bf16[2048,128]{1,0:T(8,128)(2,1)S(1)} collective-permute-done((bf16[2048,128]{1,0:T(8,128)(2,1)}, bf16[2048,128]{1,0:T(8,128)(2,1)S(1)}, u32[]{:S(2)}, u32[]{:S(2)}) %collective-permute-start.13) | collective-permute-done | bytes 524320 | tf_op jit(solution)/shard_map/ppermute | solution.py:31
  21.0 1.2 collective-permute-start.8
  22.3 1.0 copy-done.5
  23.3 1.7 %collective-permute-start = (bf16[544,512]{1,0:T(8,128)(2,1)S(1)}, bf16[544,512]{1,0:T(8,128)(2,1)S(1)}, u32[]{:S(2)}, u32[]{:S(2)}) collective-permute-start(bf16[544,512]{1,0:T(8,128)(2,1)S(1)} %get-tuple-element.18), channel_id=1, source_target_pairs={{0,64},{16,80},{32,96},{48,112},{64,128},{80,144},{96,160},{112,17... | collective-permute-start | bytes 1671176 | tf_op jit(solution)/shard_map/ppermute | solution.py:38
  25.0 1.5 %collective-permute-start.2 = (bf16[544,512]{1,0:T(8,128)(2,1)S(1)}, bf16[544,512]{1,0:T(8,128)(2,1)}, u32[]{:S(2)}, u32[]{:S(2)}) collective-permute-start(bf16[544,512]{1,0:T(8,128)(2,1)S(1)} %get-tuple-element.19), channel_id=1, source_target_pairs={{0,192},{16,208},{32,224},{48,240},{64,0},{80,16},{96,32},{112,48}... | collective-permute-start | bytes 1671176 | tf_op jit(solution)/shard_map/ppermute | solution.py:38
  26.5 4.6 %collective-permute-done.14.refs_0_ = bf16[2048,128]{1,0:T(8,128)(2,1)S(1)} collective-permute-done((bf16[2048,128]{1,0:T(8,128)(2,1)S(1)}, bf16[2048,128]{1,0:T(8,128)(2,1)S(1)}, u32[]{:S(2)}, u32[]{:S(2)}) %collective-permute-start.14) | collective-permute-done | bytes 524320 | tf_op jit(solution)/shard_map/ppermute | solution.py:31
  31.1 1.6 %collective-permute-start.4 = (bf16[544,512]{1,0:T(8,128)(2,1)S(1)}, bf16[544,512]{1,0:T(8,128)(2,1)S(1)}, u32[]{:S(2)}, u32[]{:S(2)}) collective-permute-start(bf16[544,512]{1,0:T(8,128)(2,1)S(1)} %get-tuple-element.19), channel_id=1, source_target_pairs={{0,64},{16,80},{32,96},{48,112},{64,128},{80,144},{96,160},{112,17... | collective-permute-start | bytes 1671176 | tf_op jit(solution)/shard_map/ppermute | solution.py:38
  32.7 4.0 %collective-permute-done.18.refs_1_ = bf16[2048,128]{1,0:T(8,128)(2,1)S(1)} collective-permute-done((bf16[2048,128]{1,0:T(8,128)(2,1)S(1)}, bf16[2048,128]{1,0:T(8,128)(2,1)S(1)}, u32[]{:S(2)}, u32[]{:S(2)}) %collective-permute-start.18) | collective-permute-done | bytes 524320 | tf_op jit(solution)/shard_map/ppermute | solution.py:31
  36.7 3.0 %collective-permute-start.5 = (bf16[544,512]{1,0:T(8,128)(2,1)S(1)}, bf16[544,512]{1,0:T(8,128)(2,1)S(1)}, u32[]{:S(2)}, u32[]{:S(2)}) collective-permute-start(bf16[544,512]{1,0:T(8,128)(2,1)S(1)} %get-tuple-element.18), channel_id=1, source_target_pairs={{0,192},{16,208},{32,224},{48,240},{64,0},{80,16},{96,32},{112,48}... | collective-permute-start | bytes 1671176 | tf_op jit(solution)/shard_map/ppermute | solution.py:38
  39.9 2.0 %collective-permute-done.4.refs_2_ = bf16[544,512]{1,0:T(8,128)(2,1)S(1)} collective-permute-done((bf16[544,512]{1,0:T(8,128)(2,1)S(1)}, bf16[544,512]{1,0:T(8,128)(2,1)S(1)}, u32[]{:S(2)}, u32[]{:S(2)}) %collective-permute-start.4) | collective-permute-done | bytes 557088 | tf_op jit(solution)/shard_map/ppermute | solution.py:38
  42.2 4.6 %collective-permute-done.5.refs_3_ = bf16[544,512]{1,0:T(8,128)(2,1)S(1)} collective-permute-done((bf16[544,512]{1,0:T(8,128)(2,1)S(1)}, bf16[544,512]{1,0:T(8,128)(2,1)S(1)}, u32[]{:S(2)}, u32[]{:S(2)}) %collective-permute-start.5) | collective-permute-done | bytes 557088 | tf_op jit(solution)/shard_map/ppermute | solution.py:38
  46.8 3.7 %collective-permute-start.3 = (bf16[544,512]{1,0:T(8,128)(2,1)}, bf16[544,512]{1,0:T(8,128)(2,1)}, u32[]{:S(2)}, u32[]{:S(2)}) collective-permute-start(bf16[544,512]{1,0:T(8,128)(2,1)} %collective-permute-done.2.refs_4_), channel_id=1, source_target_pairs={{0,192},{16,208},{32,224},{48,240},{64,0},{80,16},{96,32},{112,48}... | collective-permute-start | bytes 1671176 | tf_op jit(solution)/shard_map/ppermute | solution.py:38
  51.3 4.4 %collective-permute-done.19.refs_1_ = bf16[2048,128]{1,0:T(8,128)(2,1)S(1)} collective-permute-done((bf16[2048,128]{1,0:T(8,128)(2,1)S(1)}, bf16[2048,128]{1,0:T(8,128)(2,1)S(1)}, u32[]{:S(2)}, u32[]{:S(2)}) %collective-permute-start.19) | collective-permute-done | bytes 524320 | tf_op jit(solution)/shard_map/ppermute | solution.py:31
  56.6 1.0 copy-done.3
  62.1 1.2 copy-done.6
  63.3 1.1 copy-done.8
  64.4 1.1 copy-done.10
  65.4 1.1 copy-done.12
  66.5 1.5 %hold.4.refs_2_ = bf16[4,1088,512]{2,1,0:T(8,128)(2,1)S(1)} custom-call(s32[1]{0:T(128)S(6)} %select_n.7.place_ref, bf16[1088,512]{1,0:T(8,128)(2,1)S(1)} %copy-done.6, bf16[544,512]{1,0:T(8,128)(2,1)S(1)} %copy-done.8, bf16[544,512]{1,0:T(8,128)(2,1)S(1)} %copy-done.10, bf16[544,512]{1,0:T(8,128)(2,1)S(1)} %copy-done.12, ...), custom_call_target="tpu_custom_call" | custom-call | tf_op jit(solution)/shard_map/hold/pallas_call | solution.py:140
  68.0 1.4 %hold.5.refs_1_.refs_2_ = bf16[4,1088,512]{2,1,0:T(8,128)(2,1)S(1)} custom-call(s32[1]{0:T(128)S(6)} %select_n.7.place_ref, bf16[544,512]{1,0:T(8,128)(2,1)} %collective-permute-done.1.refs_0_, bf16[544,512]{1,0:T(8,128)(2,1)} %collective-permute-done.3.refs_1_, bf16[4,1088,512]{2,1,0:T(8,128)(2,1)S(1)} %hold.4.refs_2_), custom_call_target="tpu_custom_call", output_to_operand_aliasing={{}: (3, {})} | custom-call | tf_op jit(solution)/shard_map/hold/pallas_call | solution.py:140
  70.0 1.5 %hold.6.refs_2_ = bf16[4,1088,512]{2,1,0:T(8,128)(2,1)S(1)} custom-call(s32[1]{0:T(128)S(6)} %select_n.8.place_ref, bf16[1088,512]{1,0:T(8,128)(2,1)S(1)} %copy-done.4, bf16[544,512]{1,0:T(8,128)(2,1)S(1)} %copy-done.14, bf16[544,512]{1,0:T(8,128)(2,1)S(1)} %copy-done.16, bf16[544,512]{1,0:T(8,128)(2,1)S(1)} %copy-done.18, ...), custom_call_target="tpu_custom_call" | custom-call | tf_op jit(solution)/shard_map/hold/pallas_call | solution.py:140
  71.6 5.6 %collective-permute-done.20.refs_1_ = bf16[2048,128]{1,0:T(8,128)(2,1)S(1)} collective-permute-done((bf16[2048,128]{1,0:T(8,128)(2,1)S(1)}, bf16[2048,128]{1,0:T(8,128)(2,1)S(1)}, u32[]{:S(2)}, u32[]{:S(2)}) %collective-permute-start.20) | collective-permute-done | bytes 524320 | tf_op jit(solution)/shard_map/ppermute | solution.py:31
  77.2 1.0 shard_map.57.refs_4_
  78.3 1.2 hold.7.refs_2_.refs_3_
  79.5 2.8 %shard_map.58 = (bf16[2048,128]{1,0:T(8,128)(2,1)S(1)}, bf16[2048,128]{1,0:T(8,128)(2,1)S(1)}) custom-call(s32[1]{0:T(128)} %bitcast.core_ref, bf16[2048,128]{1,0:T(8,128)(2,1)S(1)} %collective-permute-done.16.refs_0_, bf16[2048,128]{1,0:T(8,128)(2,1)S(1)} %collective-permute-done.20.refs_1_, bf16[4,1088,512]{2,1,0:T(8,128)(2,1)S(1)} %hold.5.refs_1_.refs_2_, ...), custom_call_target="tpu_custom_call" | custom-call | tf_op jit(solution)/shard_map/pallas_call | solution.py:200
  82.5 1.0 shard_map.59.refs_4_
  83.5 2.8 %shard_map.60 = (f32[2048,128]{1,0:T(8,128)S(1)}, f32[2048,128]{1,0:T(8,128)S(1)}) custom-call(s32[1]{0:T(128)} %bitcast.core_ref, bf16[2048,128]{1,0:T(8,128)(2,1)S(1)} %collective-permute-done.15.refs_0_, bf16[2048,128]{1,0:T(8,128)(2,1)S(1)} %collective-permute-done.19.refs_1_, bf16[4,1088,512]{2,1,0:T(8,128)(2,1)S(1)} %hold.5.refs_1_.refs_2_, ...), custom_call_target="tpu_custom_call" | custom-call | tf_op jit(solution)/shard_map/pallas_call | solution.py:200
  86.3 5.3 %collective-permute-done.21 = bf16[2048,128]{1,0:T(8,128)(2,1)S(1)} collective-permute-done((bf16[2048,128]{1,0:T(8,128)(2,1)S(1)}, bf16[2048,128]{1,0:T(8,128)(2,1)S(1)}, u32[]{:S(2)}, u32[]{:S(2)}) %collective-permute-start.21) | collective-permute-done | bytes 524320 | tf_op jit(solution)/shard_map/ppermute | solution.py:31
  91.7 1.3 %collective-permute-start.22 = (bf16[2048,128]{1,0:T(8,128)(2,1)S(1)}, bf16[2048,128]{1,0:T(8,128)(2,1)S(1)}, u32[]{:S(2)}, u32[]{:S(2)}) collective-permute-start(bf16[2048,128]{1,0:T(8,128)(2,1)S(1)} %add_convert_fusion.4), channel_id=1, source_target_pairs={{0,14},{1,3},{2,0},{3,5},{4,2},{5,7},{6,4},{7,9},{8,6},{9,11},{10,... | collective-permute-start | bytes 1572872 | tf_op jit(solution)/shard_map/ppermute | solution.py:31
  93.0 4.2 %collective-permute-done.25 = bf16[2048,128]{1,0:T(8,128)(2,1)S(1)} collective-permute-done((bf16[2048,128]{1,0:T(8,128)(2,1)S(1)}, bf16[2048,128]{1,0:T(8,128)(2,1)S(1)}, u32[]{:S(2)}, u32[]{:S(2)}) %collective-permute-start.25) | collective-permute-done | bytes 524320 | tf_op jit(solution)/shard_map/ppermute | solution.py:31
  97.3 1.5 %collective-permute-start.26 = (bf16[2048,128]{1,0:T(8,128)(2,1)S(1)}, bf16[2048,128]{1,0:T(8,128)(2,1)S(1)}, u32[]{:S(2)}, u32[]{:S(2)}) collective-permute-start(bf16[2048,128]{1,0:T(8,128)(2,1)S(1)} %add_convert_fusion.1), channel_id=1, source_target_pairs={{0,14},{1,3},{2,0},{3,5},{4,2},{5,7},{6,4},{7,9},{8,6},{9,11},{10,... | collective-permute-start | bytes 1572872 | tf_op jit(solution)/shard_map/ppermute | solution.py:31
  98.8 1.0 shard_map.61.refs_4_
  99.8 2.8 %shard_map.62 = (f32[2048,128]{1,0:T(8,128)S(1)}, f32[2048,128]{1,0:T(8,128)S(1)}) custom-call(s32[1]{0:T(128)} %bitcast.core_ref, bf16[2048,128]{1,0:T(8,128)(2,1)S(1)} %collective-permute-done.14.refs_0_, bf16[2048,128]{1,0:T(8,128)(2,1)S(1)} %collective-permute-done.18.refs_1_, bf16[4,1088,512]{2,1,0:T(8,128)(2,1)S(1)} %hold.5.refs_1_.refs_2_, ...), custom_call_target="tpu_custom_call" | custom-call | tf_op jit(solution)/shard_map/pallas_call | solution.py:200
  102.9 1.3 %collective-permute-start.23 = (bf16[2048,128]{1,0:T(8,128)(2,1)S(1)}, bf16[2048,128]{1,0:T(8,128)(2,1)S(1)}, u32[]{:S(2)}, u32[]{:S(2)}) collective-permute-start(bf16[2048,128]{1,0:T(8,128)(2,1)S(1)} %add_convert_fusion.3), channel_id=1, source_target_pairs={{0,14},{1,3},{2,0},{3,5},{4,2},{5,7},{6,4},{7,9},{8,6},{9,11},{10,... | collective-permute-start | bytes 1572872 | tf_op jit(solution)/shard_map/ppermute | solution.py:31
  104.2 4.2 %collective-permute-done.26 = bf16[2048,128]{1,0:T(8,128)(2,1)S(1)} collective-permute-done((bf16[2048,128]{1,0:T(8,128)(2,1)S(1)}, bf16[2048,128]{1,0:T(8,128)(2,1)S(1)}, u32[]{:S(2)}, u32[]{:S(2)}) %collective-permute-start.26) | collective-permute-done | bytes 524320 | tf_op jit(solution)/shard_map/ppermute | solution.py:31
  108.5 1.3 %collective-permute-start.27 = (bf16[2048,128]{1,0:T(8,128)(2,1)S(1)}, bf16[2048,128]{1,0:T(8,128)(2,1)S(1)}, u32[]{:S(2)}, u32[]{:S(2)}) collective-permute-start(bf16[2048,128]{1,0:T(8,128)(2,1)S(1)} %add_convert_fusion), channel_id=1, source_target_pairs={{0,14},{1,3},{2,0},{3,5},{4,2},{5,7},{6,4},{7,9},{8,6},{9,11},{10,... | collective-permute-start | bytes 1572872 | tf_op jit(solution)/shard_map/ppermute | solution.py:31
  109.8 0.9 shard_map.63.refs_3_
  110.8 2.4 %shard_map.64 = f32[2048,128]{1,0:T(8,128)S(1)} custom-call(s32[1]{0:T(128)} %bitcast.core_ref, bf16[2048,128]{1,0:T(8,128)(2,1)S(1)} %copy-done.2, bf16[4,1088,512]{2,1,0:T(8,128)(2,1)S(1)} %hold.5.refs_1_.refs_2_, bf16[4,1088,512]{2,1,0:T(8,128)(2,1)S(1)} %hold.7.refs_2_.refs_3_, bf16[352,128]{1,0:T(8,128)(2,1)S(1)} %shard_map.63.refs_3_), custom_call_target="tpu_custom_call" | custom-call | tf_op jit(solution)/shard_map/pallas_call | solution.py:200
  114.2 1.3 %collective-permute-start.24 = (bf16[2048,128]{1,0:T(8,128)(2,1)S(1)}, bf16[2048,128]{1,0:T(8,128)(2,1)S(1)}, u32[]{:S(2)}, u32[]{:S(2)}) collective-permute-start(bf16[2048,128]{1,0:T(8,128)(2,1)S(1)} %add_convert_fusion.2), channel_id=1, source_target_pairs={{0,14},{1,3},{2,0},{3,5},{4,2},{5,7},{6,4},{7,9},{8,6},{9,11},{10,... | collective-permute-start | bytes 1572872 | tf_op jit(solution)/shard_map/ppermute | solution.py:31
  115.5 4.2 %collective-permute-done.27 = bf16[2048,128]{1,0:T(8,128)(2,1)S(1)} collective-permute-done((bf16[2048,128]{1,0:T(8,128)(2,1)S(1)}, bf16[2048,128]{1,0:T(8,128)(2,1)S(1)}, u32[]{:S(2)}, u32[]{:S(2)}) %collective-permute-start.27) | collective-permute-done | bytes 524320 | tf_op jit(solution)/shard_map/ppermute | solution.py:31
  119.7 0.9 shard_map.55.refs_3_
  120.6 2.4 %shard_map.56.own = f32[2048,128]{1,0:T(8,128)S(1)} custom-call(s32[1]{0:T(128)} %bitcast.core_ref, bf16[2048,128]{1,0:T(8,128)(2,1)S(1)} %copy-done, bf16[4,1088,512]{2,1,0:T(8,128)(2,1)S(1)} %hold.5.refs_1_.refs_2_, bf16[4,1088,512]{2,1,0:T(8,128)(2,1)S(1)} %hold.7.refs_2_.refs_3_, bf16[352,128]{1,0:T(8,128)(2,1)S(1)} %shard_map.55.refs_3_), custom_call_target="tpu_custom_call" | custom-call | tf_op jit(solution)/shard_map/pallas_call | solution.py:200
  123.1 2.2 %collective-permute-done.24.first = bf16[2048,128]{1,0:T(8,128)(2,1)S(1)} collective-permute-done((bf16[2048,128]{1,0:T(8,128)(2,1)S(1)}, bf16[2048,128]{1,0:T(8,128)(2,1)S(1)}, u32[]{:S(2)}, u32[]{:S(2)}) %collective-permute-start.24) | collective-permute-done | bytes 524320 | tf_op jit(solution)/shard_map/ppermute | solution.py:31
  125.3 1.0 close.1
  (72 shorter events, 9.4 us)
Async XLA Ops:
  2.7 18.1 %all-to-all-start = ((bf16[4,1088,128]{2,1,0:T(8,128)(2,1)}), bf16[4,1088,128]{2,1,0:T(8,128)(2,1)S(1)}, u32[]{:S(2)}, u32[]{:S(2)}) async-start(bf16[4,1088,128]{2,1,0:T(8,128)(2,1)} %get-tuple-element.17), calls=%async_computation | async-start | bytes 2228224 | tf_op jit(solution)/shard_map/all_to_all | solution.py:46
  8.4 12.3 %collective-permute-start.13 = (bf16[2048,128]{1,0:T(8,128)(2,1)}, bf16[2048,128]{1,0:T(8,128)(2,1)S(1)}, u32[]{:S(2)}, u32[]{:S(2)}) collective-permute-start(bf16[2048,128]{1,0:T(8,128)(2,1)} %get-tuple-element.16.refs_0_), channel_id=1, source_target_pairs={{0,2},{1,15},{2,4},{3,1},{4,6},{5,3},{6,8},{7,5},{8,10},{9,7},{10,... | collective-permute-start | bytes 1572872 | tf_op jit(solution)/shard_map/ppermute | solution.py:31
  9.4 13.9 %collective-permute-start.17 = (bf16[2048,128]{1,0:T(8,128)(2,1)}, bf16[2048,128]{1,0:T(8,128)(2,1)S(1)}, u32[]{:S(2)}, u32[]{:S(2)}) collective-permute-start(bf16[2048,128]{1,0:T(8,128)(2,1)} %get-tuple-element.16.refs_0_), channel_id=1, source_target_pairs={{0,1},{1,0},{2,3},{3,2},{4,5},{5,4},{6,7},{7,6},{8,9},{9,8},{10,11... | collective-permute-start | bytes 1572872 | tf_op jit(solution)/shard_map/ppermute | solution.py:42
  20.7 19.0 %copy-start.1 = (bf16[2048,128]{1,0:T(8,128)(2,1)}, bf16[2048,128]{1,0:T(8,128)(2,1)S(1)}, u32[]{:S(2)}) copy-start(bf16[2048,128]{1,0:T(8,128)(2,1)S(1)} %collective-permute-done.13.refs_0_) | copy-start | bytes 1572868
  20.7 10.4 %collective-permute-start.14 = (bf16[2048,128]{1,0:T(8,128)(2,1)S(1)}, bf16[2048,128]{1,0:T(8,128)(2,1)S(1)}, u32[]{:S(2)}, u32[]{:S(2)}) collective-permute-start(bf16[2048,128]{1,0:T(8,128)(2,1)S(1)} %collective-permute-done.13.refs_0_), channel_id=1, source_target_pairs={{0,2},{1,15},{2,4},{3,1},{4,6},{5,3},{6,8},{7,5},{8,10},{9,7},{10,... | collective-permute-start | bytes 1572872 | tf_op jit(solution)/shard_map/ppermute | solution.py:31
  21.0 35.5 %collective-permute-start.8 = (bf16[1088,512]{1,0:T(8,128)(2,1)S(1)}, bf16[1088,512]{1,0:T(8,128)(2,1)S(1)}, u32[]{:S(2)}, u32[]{:S(2)}) collective-permute-start(bf16[1088,512]{1,0:T(8,128)(2,1)S(1)} %get-tuple-element.20.refs_0_), channel_id=1, source_target_pairs={{0,1},{1,0},{2,3},{3,2},{4,5},{5,4},{6,7},{7,6},{8,9},{9,8},{10,11... | collective-permute-start | bytes 3342344 | tf_op jit(solution)/shard_map/ppermute | solution.py:42
  22.2 1.0 copy-start.5
  23.3 13.4 %collective-permute-start.18 = (bf16[2048,128]{1,0:T(8,128)(2,1)S(1)}, bf16[2048,128]{1,0:T(8,128)(2,1)S(1)}, u32[]{:S(2)}, u32[]{:S(2)}) collective-permute-start(bf16[2048,128]{1,0:T(8,128)(2,1)S(1)} %collective-permute-done.17), channel_id=1, source_target_pairs={{0,2},{1,15},{2,4},{3,1},{4,6},{5,3},{6,8},{7,5},{8,10},{9,7},{10,... | collective-permute-start | bytes 1572872 | tf_op jit(solution)/shard_map/ppermute | solution.py:31
  23.3 16.5 %collective-permute-start = (bf16[544,512]{1,0:T(8,128)(2,1)S(1)}, bf16[544,512]{1,0:T(8,128)(2,1)S(1)}, u32[]{:S(2)}, u32[]{:S(2)}) collective-permute-start(bf16[544,512]{1,0:T(8,128)(2,1)S(1)} %get-tuple-element.18), channel_id=1, source_target_pairs={{0,64},{16,80},{32,96},{48,112},{64,128},{80,144},{96,160},{112,17... | collective-permute-start | bytes 1671176 | tf_op jit(solution)/shard_map/ppermute | solution.py:38
  25.0 14.7 %collective-permute-start.2 = (bf16[544,512]{1,0:T(8,128)(2,1)S(1)}, bf16[544,512]{1,0:T(8,128)(2,1)}, u32[]{:S(2)}, u32[]{:S(2)}) collective-permute-start(bf16[544,512]{1,0:T(8,128)(2,1)S(1)} %get-tuple-element.19), channel_id=1, source_target_pairs={{0,192},{16,208},{32,224},{48,240},{64,0},{80,16},{96,32},{112,48}... | collective-permute-start | bytes 1671176 | tf_op jit(solution)/shard_map/ppermute | solution.py:38
  31.1 10.7 %collective-permute-start.4 = (bf16[544,512]{1,0:T(8,128)(2,1)S(1)}, bf16[544,512]{1,0:T(8,128)(2,1)S(1)}, u32[]{:S(2)}, u32[]{:S(2)}) collective-permute-start(bf16[544,512]{1,0:T(8,128)(2,1)S(1)} %get-tuple-element.19), channel_id=1, source_target_pairs={{0,64},{16,80},{32,96},{48,112},{64,128},{80,144},{96,160},{112,17... | collective-permute-start | bytes 1671176 | tf_op jit(solution)/shard_map/ppermute | solution.py:38
  36.7 10.1 %collective-permute-start.5 = (bf16[544,512]{1,0:T(8,128)(2,1)S(1)}, bf16[544,512]{1,0:T(8,128)(2,1)S(1)}, u32[]{:S(2)}, u32[]{:S(2)}) collective-permute-start(bf16[544,512]{1,0:T(8,128)(2,1)S(1)} %get-tuple-element.18), channel_id=1, source_target_pairs={{0,192},{16,208},{32,224},{48,240},{64,0},{80,16},{96,32},{112,48}... | collective-permute-start | bytes 1671176 | tf_op jit(solution)/shard_map/ppermute | solution.py:38
  39.8 10.7 %collective-permute-start.15 = (bf16[2048,128]{1,0:T(8,128)(2,1)S(1)}, bf16[2048,128]{1,0:T(8,128)(2,1)S(1)}, u32[]{:S(2)}, u32[]{:S(2)}) collective-permute-start(bf16[2048,128]{1,0:T(8,128)(2,1)S(1)} %collective-permute-done.14.refs_0_), channel_id=1, source_target_pairs={{0,2},{1,15},{2,4},{3,1},{4,6},{5,3},{6,8},{7,5},{8,10},{9,7},{10,... | collective-permute-start | bytes 1572872 | tf_op jit(solution)/shard_map/ppermute | solution.py:31
  39.8 16.0 %collective-permute-start.19 = (bf16[2048,128]{1,0:T(8,128)(2,1)S(1)}, bf16[2048,128]{1,0:T(8,128)(2,1)S(1)}, u32[]{:S(2)}, u32[]{:S(2)}) collective-permute-start(bf16[2048,128]{1,0:T(8,128)(2,1)S(1)} %collective-permute-done.18.refs_1_), channel_id=1, source_target_pairs={{0,2},{1,15},{2,4},{3,1},{4,6},{5,3},{6,8},{7,5},{8,10},{9,7},{10,... | collective-permute-start | bytes 1572872 | tf_op jit(solution)/shard_map/ppermute | solution.py:31
  41.9 17.0 %collective-permute-start.1 = (bf16[544,512]{1,0:T(8,128)(2,1)S(1)}, bf16[544,512]{1,0:T(8,128)(2,1)}, u32[]{:S(2)}, u32[]{:S(2)}) collective-permute-start(bf16[544,512]{1,0:T(8,128)(2,1)S(1)} %collective-permute-done.refs_1_), channel_id=1, source_target_pairs={{0,64},{16,80},{32,96},{48,112},{64,128},{80,144},{96,160},{112,17... | collective-permute-start | bytes 1671176 | tf_op jit(solution)/shard_map/ppermute | solution.py:38
  46.8 12.1 %collective-permute-start.3 = (bf16[544,512]{1,0:T(8,128)(2,1)}, bf16[544,512]{1,0:T(8,128)(2,1)}, u32[]{:S(2)}, u32[]{:S(2)}) collective-permute-start(bf16[544,512]{1,0:T(8,128)(2,1)} %collective-permute-done.2.refs_4_), channel_id=1, source_target_pairs={{0,192},{16,208},{32,224},{48,240},{64,0},{80,16},{96,32},{112,48}... | collective-permute-start | bytes 1671176 | tf_op jit(solution)/shard_map/ppermute | solution.py:38
  50.5 8.9 %collective-permute-start.9 = (bf16[544,512]{1,0:T(8,128)(2,1)S(1)}, bf16[544,512]{1,0:T(8,128)(2,1)S(1)}, u32[]{:S(2)}, u32[]{:S(2)}) collective-permute-start(bf16[544,512]{1,0:T(8,128)(2,1)S(1)} %collective-permute-done.refs_1_), channel_id=1, source_target_pairs={{0,1},{1,0},{2,3},{3,2},{4,5},{5,4},{6,7},{7,6},{8,9},{9,8},{10,11... | collective-permute-start | bytes 1671176 | tf_op jit(solution)/shard_map/ppermute | solution.py:42
  50.5 0.8 copy-start.7
  55.8 4.6 %collective-permute-start.10 = (bf16[544,512]{1,0:T(8,128)(2,1)S(1)}, bf16[544,512]{1,0:T(8,128)(2,1)S(1)}, u32[]{:S(2)}, u32[]{:S(2)}) collective-permute-start(bf16[544,512]{1,0:T(8,128)(2,1)S(1)} %collective-permute-done.4.refs_2_), channel_id=1, source_target_pairs={{0,1},{1,0},{2,3},{3,2},{4,5},{5,4},{6,7},{7,6},{8,9},{9,8},{10,11... | collective-permute-start | bytes 1671176 | tf_op jit(solution)/shard_map/ppermute | solution.py:42
  56.6 1.0 copy-start.3
  57.6 3.7 %collective-permute-start.11 = (bf16[544,512]{1,0:T(8,128)(2,1)S(1)}, bf16[544,512]{1,0:T(8,128)(2,1)S(1)}, u32[]{:S(2)}, u32[]{:S(2)}) collective-permute-start(bf16[544,512]{1,0:T(8,128)(2,1)S(1)} %collective-permute-done.5.refs_3_), channel_id=1, source_target_pairs={{0,1},{1,0},{2,3},{3,2},{4,5},{5,4},{6,7},{7,6},{8,9},{9,8},{10,11... | collective-permute-start | bytes 1671176 | tf_op jit(solution)/shard_map/ppermute | solution.py:42
  58.1 0.8 copy-start.11
  58.9 10.5 %collective-permute-start.12 = (bf16[544,512]{1,0:T(8,128)(2,1)}, bf16[544,512]{1,0:T(8,128)(2,1)}, u32[]{:S(2)}, u32[]{:S(2)}) collective-permute-start(bf16[544,512]{1,0:T(8,128)(2,1)} %collective-permute-done.2.refs_4_), channel_id=1, source_target_pairs={{0,1},{1,0},{2,3},{3,2},{4,5},{5,4},{6,7},{7,6},{8,9},{9,8},{10,11... | collective-permute-start | bytes 1671176 | tf_op jit(solution)/shard_map/ppermute | solution.py:42
  58.9 19.3 %collective-permute-start.6 = (bf16[544,512]{1,0:T(8,128)(2,1)}, bf16[544,512]{1,0:T(8,128)(2,1)}, u32[]{:S(2)}, u32[]{:S(2)}) collective-permute-start(bf16[544,512]{1,0:T(8,128)(2,1)} %collective-permute-done.1.refs_0_), channel_id=1, source_target_pairs={{0,1},{1,0},{2,3},{3,2},{4,5},{5,4},{6,7},{7,6},{8,9},{9,8},{10,11... | collective-permute-start | bytes 1671176 | tf_op jit(solution)/shard_map/ppermute | solution.py:42
  59.4 0.9 copy-start.13
  60.3 18.0 %collective-permute-start.7 = (bf16[544,512]{1,0:T(8,128)(2,1)}, bf16[544,512]{1,0:T(8,128)(2,1)}, u32[]{:S(2)}, u32[]{:S(2)}) collective-permute-start(bf16[544,512]{1,0:T(8,128)(2,1)} %collective-permute-done.3.refs_1_), channel_id=1, source_target_pairs={{0,1},{1,0},{2,3},{3,2},{4,5},{5,4},{6,7},{7,6},{8,9},{9,8},{10,11... | collective-permute-start | bytes 1671176 | tf_op jit(solution)/shard_map/ppermute | solution.py:42
  60.4 0.9 copy-start.15
  61.2 10.4 %collective-permute-start.16 = (bf16[2048,128]{1,0:T(8,128)(2,1)S(1)}, bf16[2048,128]{1,0:T(8,128)(2,1)S(1)}, u32[]{:S(2)}, u32[]{:S(2)}) collective-permute-start(bf16[2048,128]{1,0:T(8,128)(2,1)S(1)} %collective-permute-done.15.refs_0_), channel_id=1, source_target_pairs={{0,2},{1,15},{2,4},{3,1},{4,6},{5,3},{6,8},{7,5},{8,10},{9,7},{10,... | collective-permute-start | bytes 1572872 | tf_op jit(solution)/shard_map/ppermute | solution.py:31
  61.2 0.8 copy-start.17
  62.1 15.2 %collective-permute-start.20 = (bf16[2048,128]{1,0:T(8,128)(2,1)S(1)}, bf16[2048,128]{1,0:T(8,128)(2,1)S(1)}, u32[]{:S(2)}, u32[]{:S(2)}) collective-permute-start(bf16[2048,128]{1,0:T(8,128)(2,1)S(1)} %collective-permute-done.19.refs_1_), channel_id=1, source_target_pairs={{0,2},{1,15},{2,4},{3,1},{4,6},{5,3},{6,8},{7,5},{8,10},{9,7},{10,... | collective-permute-start | bytes 1572872 | tf_op jit(solution)/shard_map/ppermute | solution.py:31
  62.1 1.2 copy-start.6
  63.3 1.1 copy-start.8
  64.4 1.1 copy-start.10
  65.4 1.1 copy-start.12
  68.0 1.6 %copy-start.4 = (bf16[1088,512]{1,0:T(8,128)(2,1)S(1)}, bf16[1088,512]{1,0:T(8,128)(2,1)}, u32[]{:S(2)}) copy-start(bf16[1088,512]{1,0:T(8,128)(2,1)} %copy-done.3) | copy-start | bytes 3342340
  68.0 1.7 %copy-start.14 = (bf16[544,512]{1,0:T(8,128)(2,1)S(1)}, bf16[544,512]{1,0:T(8,128)(2,1)}, u32[]{:S(2)}) copy-start(bf16[544,512]{1,0:T(8,128)(2,1)} %copy-done.13) | copy-start | bytes 1671172
  68.0 1.9 %copy-start.16 = (bf16[544,512]{1,0:T(8,128)(2,1)S(1)}, bf16[544,512]{1,0:T(8,128)(2,1)}, u32[]{:S(2)}) copy-start(bf16[544,512]{1,0:T(8,128)(2,1)} %copy-done.15) | copy-start | bytes 1671172
  68.0 2.0 %copy-start.18 = (bf16[544,512]{1,0:T(8,128)(2,1)S(1)}, bf16[544,512]{1,0:T(8,128)(2,1)}, u32[]{:S(2)}) copy-start(bf16[544,512]{1,0:T(8,128)(2,1)} %copy-done.17) | copy-start | bytes 1671172
  82.3 9.3 %collective-permute-start.21 = (bf16[2048,128]{1,0:T(8,128)(2,1)S(1)}, bf16[2048,128]{1,0:T(8,128)(2,1)S(1)}, u32[]{:S(2)}, u32[]{:S(2)}) collective-permute-start(bf16[2048,128]{1,0:T(8,128)(2,1)S(1)} %get-tuple-element.21), channel_id=1, source_target_pairs={{0,14},{1,3},{2,0},{3,5},{4,2},{5,7},{6,4},{7,9},{8,6},{9,11},{10,... | collective-permute-start | bytes 1572872 | tf_op jit(solution)/shard_map/ppermute | solution.py:31
  82.4 14.8 %collective-permute-start.25 = (bf16[2048,128]{1,0:T(8,128)(2,1)S(1)}, bf16[2048,128]{1,0:T(8,128)(2,1)S(1)}, u32[]{:S(2)}, u32[]{:S(2)}) collective-permute-start(bf16[2048,128]{1,0:T(8,128)(2,1)S(1)} %get-tuple-element.24), channel_id=1, source_target_pairs={{0,14},{1,3},{2,0},{3,5},{4,2},{5,7},{6,4},{7,9},{8,6},{9,11},{10,... | collective-permute-start | bytes 1572872 | tf_op jit(solution)/shard_map/ppermute | solution.py:31
  91.7 11.1 %collective-permute-start.22 = (bf16[2048,128]{1,0:T(8,128)(2,1)S(1)}, bf16[2048,128]{1,0:T(8,128)(2,1)S(1)}, u32[]{:S(2)}, u32[]{:S(2)}) collective-permute-start(bf16[2048,128]{1,0:T(8,128)(2,1)S(1)} %add_convert_fusion.4), channel_id=1, source_target_pairs={{0,14},{1,3},{2,0},{3,5},{4,2},{5,7},{6,4},{7,9},{8,6},{9,11},{10,... | collective-permute-start | bytes 1572872 | tf_op jit(solution)/shard_map/ppermute | solution.py:31
  97.3 11.1 %collective-permute-start.26 = (bf16[2048,128]{1,0:T(8,128)(2,1)S(1)}, bf16[2048,128]{1,0:T(8,128)(2,1)S(1)}, u32[]{:S(2)}, u32[]{:S(2)}) collective-permute-start(bf16[2048,128]{1,0:T(8,128)(2,1)S(1)} %add_convert_fusion.1), channel_id=1, source_target_pairs={{0,14},{1,3},{2,0},{3,5},{4,2},{5,7},{6,4},{7,9},{8,6},{9,11},{10,... | collective-permute-start | bytes 1572872 | tf_op jit(solution)/shard_map/ppermute | solution.py:31
  102.6 7.2 %copy-start.2 = (bf16[2048,128]{1,0:T(8,128)(2,1)S(1)}, bf16[2048,128]{1,0:T(8,128)(2,1)}, u32[]{:S(2)}) copy-start(bf16[2048,128]{1,0:T(8,128)(2,1)} %copy-done.1) | copy-start | bytes 1572868
  102.9 11.1 %collective-permute-start.23 = (bf16[2048,128]{1,0:T(8,128)(2,1)S(1)}, bf16[2048,128]{1,0:T(8,128)(2,1)S(1)}, u32[]{:S(2)}, u32[]{:S(2)}) collective-permute-start(bf16[2048,128]{1,0:T(8,128)(2,1)S(1)} %add_convert_fusion.3), channel_id=1, source_target_pairs={{0,14},{1,3},{2,0},{3,5},{4,2},{5,7},{6,4},{7,9},{8,6},{9,11},{10,... | collective-permute-start | bytes 1572872 | tf_op jit(solution)/shard_map/ppermute | solution.py:31
  108.5 11.1 %collective-permute-start.27 = (bf16[2048,128]{1,0:T(8,128)(2,1)S(1)}, bf16[2048,128]{1,0:T(8,128)(2,1)S(1)}, u32[]{:S(2)}, u32[]{:S(2)}) collective-permute-start(bf16[2048,128]{1,0:T(8,128)(2,1)S(1)} %add_convert_fusion), channel_id=1, source_target_pairs={{0,14},{1,3},{2,0},{3,5},{4,2},{5,7},{6,4},{7,9},{8,6},{9,11},{10,... | collective-permute-start | bytes 1572872 | tf_op jit(solution)/shard_map/ppermute | solution.py:31
  110.8 8.9 %copy-start = (bf16[2048,128]{1,0:T(8,128)(2,1)S(1)}, bf16[2048,128]{1,0:T(8,128)(2,1)}, u32[]{:S(2)}) copy-start(bf16[2048,128]{1,0:T(8,128)(2,1)} %get-tuple-element.16.refs_0_) | copy-start | bytes 1572868
  114.2 11.1 %collective-permute-start.24 = (bf16[2048,128]{1,0:T(8,128)(2,1)S(1)}, bf16[2048,128]{1,0:T(8,128)(2,1)S(1)}, u32[]{:S(2)}, u32[]{:S(2)}) collective-permute-start(bf16[2048,128]{1,0:T(8,128)(2,1)S(1)} %add_convert_fusion.2), channel_id=1, source_target_pairs={{0,14},{1,3},{2,0},{3,5},{4,2},{5,7},{6,4},{7,9},{8,6},{9,11},{10,... | collective-permute-start | bytes 1572872 | tf_op jit(solution)/shard_map/ppermute | solution.py:31
  119.7 5.6 %collective-permute-start.28 = (bf16[2048,128]{1,0:T(8,128)(2,1)S(1)}, bf16[2048,128]{1,0:T(8,128)(2,1)S(1)}, u32[]{:S(2)}, u32[]{:S(2)}) collective-permute-start(bf16[2048,128]{1,0:T(8,128)(2,1)S(1)} %collective-permute-done.27), channel_id=1, source_target_pairs={{0,1},{1,0},{2,3},{3,2},{4,5},{5,4},{6,7},{7,6},{8,9},{9,8},{10,11... | collective-permute-start | bytes 1572872 | tf_op jit(solution)/shard_map/ppermute | solution.py:42
  (1 other events, 0.8 us)

commit v2 on v1

--- a/solution.py
+++ b/solution.py
@@ -171,6 +171,47 @@
     out[...] = half_hidden(core_ref[0], 0, units, pieces, weights, turned)
 
 
+def begin_far_body(n, units, core_ref, place_ref, *refs):
+    pieces, (top, bottom, _, out, weights, turned, sems) = refs[:n], refs[n:]
+    core, place, m, depth, half = core_ref[0], place_ref[0], pieces[0].shape[1], weights.shape[2], top.shape[0]
+    far = (place + 2) % 4
+    copies = [
+        pltpu.make_async_copy(top, weights.at[far, :half], sems.at[0]),
+        pltpu.make_async_copy(bottom, weights.at[far, half:], sems.at[1]),
+    ]
+    for c in copies:
+        c.start()
+    for b in range(turned.shape[0] // LANES):
+        at = pl.ds(pl.multiple_of(order(core, b, 0) * LANES, LANES), LANES)
+        for i, piece in enumerate(pieces):
+            turned[LANES * b : LANES * (b + 1), m * i : m * (i + 1)] = piece[at, :]
+    both = 0.0
+    for by in (3, 0, 1, 2):
+        if by == 2:
+            for c in copies:
+                c.wait()
+        k = (place + by) % 4
+        rows = turned[pl.ds(pl.multiple_of(k * depth, depth), depth), :]
+        both += jnp.dot(weights[k, : 2 * units], rows, preferred_element_type=f32)
+    gate, upper = both[:units], both[units:]
+    out[...] = (gate / (1.0 + jnp.exp(-gate)) * upper).astype(bf16)
+
+
+def begin_far(units, core, place, pieces, top, bottom, weights):
+    n, (features, m) = len(pieces), pieces[0].shape
+    smem, remote = pl.BlockSpec(memory_space=pltpu.SMEM), pl.BlockSpec(memory_space=pltpu.HBM)
+    return pl.pallas_call(
+        functools.partial(begin_far_body, n, units),
+        out_shape=[jax.ShapeDtypeStruct((units, n * m), bf16), jax.ShapeDtypeStruct(weights.shape, bf16)],
+        in_specs=[smem] * 2 + [WHOLE] * n + [remote] * 2 + [WHOLE],
+        out_specs=[WHOLE] * 2,
+        input_output_aliases={n + 4: 1},
+        scratch_shapes=[pltpu.VMEM((features, n * m), bf16), pltpu.SemaphoreType.DMA((2,))],
+        compiler_params=pltpu.CompilerParams(vmem_limit_bytes=18 << 20),
+        name="begin_far",
+    )(core, place, *pieces, top, bottom, weights)
+
+
 def finish_body(n, units, core_ref, *refs):
     pieces, weights, first = refs[:n], refs[n : n + 2], refs[n + 2]
     outs, turned, held = refs[n + 3 : 2 * n + 3], refs[2 * n + 3], refs[2 * n + 4]
@@ -258,17 +299,20 @@
     first = core == 0
     shape = (4, *here.shape)
 
-    def held(place, blocks):
-        most = hold(place, PARTS[:5], blocks[:5], shape)
-        return hold(place, PARTS[5:], blocks[5:], shape, most)
-
-    columns = held(jnp.where(first, row, column), blocks)
-    weights = columns, held(jnp.where(first, column, row), others)
+    def hold_most(place, blocks):
+        return hold(place, PARTS[:5], blocks[:5], shape)
 
     units = down_weight.shape[0]
     groups = [(own[4], mate[3]), (own[3], mate[2]), (own[2], mate[1]), (own[1],), (own[0],)]
-    firsts = []
-    for g in groups:
+    mine, other = jnp.where(first, row, column), jnp.where(first, column, row)
+    columns = hold_most(mine, blocks)
+    start, columns = begin_far(units, core, mine, groups[0], *blocks[5:], columns)
+    others_columns = hold_most(other, others)
+    others_columns = hold(other, PARTS[5:], others[5:], shape, others_columns)
+    weights = columns, others_columns
+
+    firsts = [start]
+    for i, g in enumerate(groups[1:], 1):
         firsts.append(begin(units, core, g, columns))
     shares = []
     for i, (g, f) in enumerate(zip(groups, firsts)):
@@ -285,7 +329,8 @@
     got_own = send(got_own.astype(f32) + own2)
     got_mate = send(got_mate.astype(f32) + mate1)
     got_own = send(got_own.astype(f32) + own1)
-    return close(own0, got_own, swap(got_mate))
+    got_mate = swap(got_mate)
+    return close(own0, got_own, got_mate)
 
 
 def solution(mesh):

time: 127 us -> 134 us (1.055)
  waiting for transfers between devices: 55 us -> 63 us
  starting transfers between devices: 30.8 us -> 28.3 us
  Pallas kernels: 27.7 us -> 29.4 us
    ppermute x14, waiting for transfers between devices: 48.4 us -> 56.8 us  [onward(): return lax.ppermute(x, ('z', 'c'), pairs)]
    pallas_call x0 -> x1, Pallas kernels: none -> 2.99 us  [begin_far(): pl.pallas_call(functools.partial(begin_far_body, n, units), out_shape=[ja...]
    ppermute x6, starting transfers between devices: 11.9 us -> 9.41 us  [along_column(): return lax.ppermute(x, ('y', 'x', 'c'), pairs)]
    pallas_call x4 -> x3, Pallas kernels: 5.61 us -> 4.23 us  [hold(): pl.pallas_call(functools.partial(hold_body, parts), out_shape=jax.ShapeDt...]
    unnamed x38 -> x34, local copies, waits for them, and re-layouts: 12 us -> 11.5 us
    pallas_call x10 -> x9, Pallas kernels: 18.1 us -> 18.2 us  [call(): pl.pallas_call(functools.partial(body, n, units), out_shape=out_shape, in...]
  transfers between devices with their start and end apart: 30 -> 30, of which waited for: 15 -> 16; matrix products, arithmetic and copies ran while one was open for 0% -> 1% of each run, Pallas kernels for 16% -> 15%
where the time goes in v2:
time: 134 us; the launch traced here: 133 us
  waiting for transfers between devices  63 us (47%)
  Pallas kernels  29.4 us (22%)
  starting transfers between devices  28.3 us (21%)
  local copies, waits for them, and re-layouts  11.5 us (9%)
    ppermute x14, waiting for transfers between devices, onward(): return lax.ppermute(x, ('z', 'c'), pairs)  56.8 us
    pallas_call x9, Pallas kernels, call(): pl.pallas_call(functools.partial(body, n, units), out_shape=out_shape, in...  18.2 us
    unnamed x34, local copies, waits for them, and re-layouts  11.5 us
    ppermute x6, starting transfers between devices, along_column(): return lax.ppermute(x, ('y', 'x', 'c'), pairs)  9.41 us
    ppermute x14, starting transfers between devices, onward(): return lax.ppermute(x, ('z', 'c'), pairs)  7.96 us
    ppermute x6, waiting for transfers between devices, along_column(): return lax.ppermute(x, ('y', 'x', 'c'), pairs)  6.25 us
    all_to_all x1, starting transfers between devices, from_four(): lax.all_to_all(copies, AXES, 0, 0, axis_index_groups=groups, tiled=True)  5.74 us
    ppermute x9, starting transfers between devices, swap(): return lax.ppermute(x, 'c', [(0, 1), (1, 0)])  5.19 us
  transfers between devices with their start and end apart: 30, of which 16 were waited for; matrix products, arithmetic and copies ran while one was open for 1% of the time, Pallas kernels for 15%

profile of v2, /device:TPU:2, one launch (start us, length us, event | category | flops | bytes accessed | tf_op | source)
XLA Modules:
  0.0 133.2 jit_solution(15176898775975629264)
XLA Ops:
  0.0 2.6 %opening.1 = (bf16[2048,128]{1,0:T(8,128)(2,1)}, bf16[4,1088,128]{2,1,0:T(8,128)(2,1)}) custom-call(bf16[128,2048]{1,0:T(8,128)(2,1)} %tokens_in.1, f32[1,2048]{1,0:T(1,128)} %bitcast.8, bf16[352,128]{1,0:T(8,128)(2,1)} %bitcast.6, bf16[352,128]{1,0:T(8,128)(2,1)} %bitcast.7, bf16[352,128]{1,0:T(8,128)(2,1)} %down_in.1), custom_call_target="tpu_custom_call" | custom-call | tf_op jit(solution)/shard_map/opening/pallas_call | solution.py:82
  2.7 5.7 %all-to-all-start = ((bf16[4,1088,128]{2,1,0:T(8,128)(2,1)}), bf16[4,1088,128]{2,1,0:T(8,128)(2,1)S(1)}, u32[]{:S(2)}, u32[]{:S(2)}) async-start(bf16[4,1088,128]{2,1,0:T(8,128)(2,1)} %get-tuple-element.19), calls=%async_computation | async-start | bytes 2228224 | tf_op jit(solution)/shard_map/all_to_all | solution.py:46
  8.4 1.0 collective-permute-start
  9.4 2.9 %collective-permute-start.4 = (bf16[2048,128]{1,0:T(8,128)(2,1)}, bf16[2048,128]{1,0:T(8,128)(2,1)S(1)}, u32[]{:S(2)}, u32[]{:S(2)}) collective-permute-start(bf16[2048,128]{1,0:T(8,128)(2,1)} %get-tuple-element.18.refs_0_), channel_id=1, source_target_pairs={{0,1},{1,0},{2,3},{3,2},{4,5},{5,4},{6,7},{7,6},{8,9},{9,8},{10,11... | collective-permute-start | bytes 1572872 | tf_op jit(solution)/shard_map/ppermute | solution.py:42
  12.3 8.5 %collective-permute-done.refs_0_ = bf16[2048,128]{1,0:T(8,128)(2,1)S(1)} collective-permute-done((bf16[2048,128]{1,0:T(8,128)(2,1)}, bf16[2048,128]{1,0:T(8,128)(2,1)S(1)}, u32[]{:S(2)}, u32[]{:S(2)}) %collective-permute-start) | collective-permute-done | bytes 524320 | tf_op jit(solution)/shard_map/ppermute | solution.py:31
  21.0 1.2 collective-permute-start.16
  22.2 1.0 copy-done.3
  23.3 3.0 %collective-permute-start.10 = (bf16[544,512]{1,0:T(8,128)(2,1)S(1)}, bf16[544,512]{1,0:T(8,128)(2,1)S(1)}, u32[]{:S(2)}, u32[]{:S(2)}) collective-permute-start(bf16[544,512]{1,0:T(8,128)(2,1)S(1)} %get-tuple-element.21), channel_id=1, source_target_pairs={{0,192},{16,208},{32,224},{48,240},{64,0},{80,16},{96,32},{112,48}... | collective-permute-start | bytes 1671176 | tf_op jit(solution)/shard_map/ppermute | solution.py:38
  26.2 4.9 %collective-permute-done.1.refs_0_ = bf16[2048,128]{1,0:T(8,128)(2,1)S(1)} collective-permute-done((bf16[2048,128]{1,0:T(8,128)(2,1)S(1)}, bf16[2048,128]{1,0:T(8,128)(2,1)S(1)}, u32[]{:S(2)}, u32[]{:S(2)}) %collective-permute-start.1) | collective-permute-done | bytes 524320 | tf_op jit(solution)/shard_map/ppermute | solution.py:31
  31.1 1.6 %collective-permute-start.12 = (bf16[544,512]{1,0:T(8,128)(2,1)S(1)}, bf16[544,512]{1,0:T(8,128)(2,1)S(1)}, u32[]{:S(2)}, u32[]{:S(2)}) collective-permute-start(bf16[544,512]{1,0:T(8,128)(2,1)S(1)} %get-tuple-element.21), channel_id=1, source_target_pairs={{0,64},{16,80},{32,96},{48,112},{64,128},{80,144},{96,160},{112,17... | collective-permute-start | bytes 1671176 | tf_op jit(solution)/shard_map/ppermute | solution.py:38
  32.7 4.0 %collective-permute-done.5.refs_1_ = bf16[2048,128]{1,0:T(8,128)(2,1)S(1)} collective-permute-done((bf16[2048,128]{1,0:T(8,128)(2,1)S(1)}, bf16[2048,128]{1,0:T(8,128)(2,1)S(1)}, u32[]{:S(2)}, u32[]{:S(2)}) %collective-permute-start.5) | collective-permute-done | bytes 524320 | tf_op jit(solution)/shard_map/ppermute | solution.py:31
  36.7 3.0 %collective-permute-start.13 = (bf16[544,512]{1,0:T(8,128)(2,1)S(1)}, bf16[544,512]{1,0:T(8,128)(2,1)}, u32[]{:S(2)}, u32[]{:S(2)}) collective-permute-start(bf16[544,512]{1,0:T(8,128)(2,1)S(1)} %get-tuple-element.20), channel_id=1, source_target_pairs={{0,192},{16,208},{32,224},{48,240},{64,0},{80,16},{96,32},{112,48}... | collective-permute-start | bytes 1671176 | tf_op jit(solution)/shard_map/ppermute | solution.py:38
  39.8 3.1 %collective-permute-done.12.refs_2_ = bf16[544,512]{1,0:T(8,128)(2,1)S(1)} collective-permute-done((bf16[544,512]{1,0:T(8,128)(2,1)S(1)}, bf16[544,512]{1,0:T(8,128)(2,1)S(1)}, u32[]{:S(2)}, u32[]{:S(2)}) %collective-permute-start.12) | collective-permute-done | bytes 557088 | tf_op jit(solution)/shard_map/ppermute | solution.py:38
  43.7 3.1 %collective-permute-done.13.refs_3_ = bf16[544,512]{1,0:T(8,128)(2,1)} collective-permute-done((bf16[544,512]{1,0:T(8,128)(2,1)S(1)}, bf16[544,512]{1,0:T(8,128)(2,1)}, u32[]{:S(2)}, u32[]{:S(2)}) %collective-permute-start.13) | collective-permute-done | bytes 557088 | tf_op jit(solution)/shard_map/ppermute | solution.py:38
  46.8 1.1 collective-permute-start.9
  47.9 2.2 %collective-permute-done.2.refs_0_ = bf16[2048,128]{1,0:T(8,128)(2,1)S(1)} collective-permute-done((bf16[2048,128]{1,0:T(8,128)(2,1)S(1)}, bf16[2048,128]{1,0:T(8,128)(2,1)S(1)}, u32[]{:S(2)}, u32[]{:S(2)}) %collective-permute-start.2) | collective-permute-done | bytes 524320 | tf_op jit(solution)/shard_map/ppermute | solution.py:31
  51.0 4.8 %collective-permute-done.6.refs_1_ = bf16[2048,128]{1,0:T(8,128)(2,1)S(1)} collective-permute-done((bf16[2048,128]{1,0:T(8,128)(2,1)S(1)}, bf16[2048,128]{1,0:T(8,128)(2,1)S(1)}, u32[]{:S(2)}, u32[]{:S(2)}) %collective-permute-start.6) | collective-permute-done | bytes 524320 | tf_op jit(solution)/shard_map/ppermute | solution.py:31
  56.6 1.0 copy-done.1
  62.1 1.3 %copy-done.4 = bf16[1088,512]{1,0:T(8,128)(2,1)S(1)} copy-done((bf16[1088,512]{1,0:T(8,128)(2,1)S(1)}, bf16[1088,512]{1,0:T(8,128)(2,1)}, u32[]{:S(2)}) %copy-start.4) | copy-done | bytes 1114136
  63.4 1.1 copy-done.6
  64.5 1.1 copy-done.8
  65.5 1.1 copy-done.10
  66.6 1.6 %hold.3.refs_4_ = bf16[4,1088,512]{2,1,0:T(8,128)(2,1)S(1)} custom-call(s32[1]{0:T(128)S(6)} %select_n.7.place_ref, bf16[1088,512]{1,0:T(8,128)(2,1)S(1)} %copy-done.4, bf16[544,512]{1,0:T(8,128)(2,1)S(1)} %copy-done.8, bf16[544,512]{1,0:T(8,128)(2,1)S(1)} %copy-done.10, bf16[544,512]{1,0:T(8,128)(2,1)} %collective-permute-done.13.refs_3_, ...), custom_call_target="tpu_custom_call" | custom-call | tf_op jit(solution)/shard_map/hold/pallas_call | solution.py:140
  68.2 1.4 %hold.4.refs_2_ = bf16[4,1088,512]{2,1,0:T(8,128)(2,1)S(1)} custom-call(s32[1]{0:T(128)S(6)} %select_n.8.place_ref, bf16[1088,512]{1,0:T(8,128)(2,1)S(1)} %copy-done.2, bf16[544,512]{1,0:T(8,128)(2,1)S(1)} %copy-done.12, bf16[544,512]{1,0:T(8,128)(2,1)S(1)} %copy-done.16, bf16[544,512]{1,0:T(8,128)(2,1)} %collective-permute-done.19.refs_3_, ...), custom_call_target="tpu_custom_call" | custom-call | tf_op jit(solution)/shard_map/hold/pallas_call | solution.py:140
  69.6 2.0 %collective-permute-done.3.refs_0_ = bf16[2048,128]{1,0:T(8,128)(2,1)S(1)} collective-permute-done((bf16[2048,128]{1,0:T(8,128)(2,1)S(1)}, bf16[2048,128]{1,0:T(8,128)(2,1)S(1)}, u32[]{:S(2)}, u32[]{:S(2)}) %collective-permute-start.3) | collective-permute-done | bytes 524320 | tf_op jit(solution)/shard_map/ppermute | solution.py:31
  71.6 5.7 %collective-permute-done.7.refs_1_ = bf16[2048,128]{1,0:T(8,128)(2,1)} collective-permute-done((bf16[2048,128]{1,0:T(8,128)(2,1)S(1)}, bf16[2048,128]{1,0:T(8,128)(2,1)}, u32[]{:S(2)}, u32[]{:S(2)}) %collective-permute-start.7) | collective-permute-done | bytes 524320 | tf_op jit(solution)/shard_map/ppermute | solution.py:31
  77.3 3.0 %begin_far.1 = (bf16[352,256]{1,0:T(8,128)(2,1)S(1)}, bf16[4,1088,512]{2,1,0:T(8,128)(2,1)S(1)}) custom-call(s32[1]{0:T(128)} %bitcast.core_ref, s32[1]{0:T(128)S(6)} %select_n.7.place_ref, bf16[2048,128]{1,0:T(8,128)(2,1)S(1)} %collective-permute-done.3.refs_0_, bf16[2048,128]{1,0:T(8,128)(2,1)} %collective-permute-done.7.refs_1_, ...), custom_call_target="tpu_custom_call", output_to_operand_aliasing={{1}: (6, {})} | custom-call | tf_op jit(solution)/shard_map/begin_far/pallas_call | solution.py:203
  80.3 1.2 hold.5.refs_2_.refs_3_
  81.6 3.8 %shard_map.57 = (bf16[2048,128]{1,0:T(8,128)(2,1)S(1)}, bf16[2048,128]{1,0:T(8,128)(2,1)S(1)}) custom-call(s32[1]{0:T(128)} %bitcast.core_ref, bf16[2048,128]{1,0:T(8,128)(2,1)S(1)} %collective-permute-done.3.refs_0_, bf16[2048,128]{1,0:T(8,128)(2,1)} %collective-permute-done.7.refs_1_, bf16[4,1088,512]{2,1,0:T(8,128)(2,1)S(1)} %get-tuple-element.23.refs_1_.refs_2_, ...), custom_call_target="tpu_custom_call" | custom-call | tf_op jit(solution)/shard_map/pallas_call | solution.py:241
  85.6 1.0 shard_map.58.refs_4_
  86.7 2.8 %shard_map.59 = (f32[2048,128]{1,0:T(8,128)S(1)}, f32[2048,128]{1,0:T(8,128)S(1)}) custom-call(s32[1]{0:T(128)} %bitcast.core_ref, bf16[2048,128]{1,0:T(8,128)(2,1)S(1)} %collective-permute-done.2.refs_0_, bf16[2048,128]{1,0:T(8,128)(2,1)S(1)} %collective-permute-done.6.refs_1_, bf16[4,1088,512]{2,1,0:T(8,128)(2,1)S(1)} %get-tuple-element.23.refs_1_.refs_2_, ...), custom_call_target="tpu_custom_call" | custom-call | tf_op jit(solution)/shard_map/pallas_call | solution.py:241
  89.4 5.3 %collective-permute-done.25 = bf16[2048,128]{1,0:T(8,128)(2,1)S(1)} collective-permute-done((bf16[2048,128]{1,0:T(8,128)(2,1)S(1)}, bf16[2048,128]{1,0:T(8,128)(2,1)S(1)}, u32[]{:S(2)}, u32[]{:S(2)}) %collective-permute-start.25) | collective-permute-done | bytes 524320 | tf_op jit(solution)/shard_map/ppermute | solution.py:31
  94.9 1.3 collective-permute-start.26
  96.1 4.2 %collective-permute-done.21 = bf16[2048,128]{1,0:T(8,128)(2,1)S(1)} collective-permute-done((bf16[2048,128]{1,0:T(8,128)(2,1)S(1)}, bf16[2048,128]{1,0:T(8,128)(2,1)S(1)}, u32[]{:S(2)}, u32[]{:S(2)}) %collective-permute-start.21) | collective-permute-done | bytes 524320 | tf_op jit(solution)/shard_map/ppermute | solution.py:31
  100.5 1.5 %collective-permute-start.22 = (bf16[2048,128]{1,0:T(8,128)(2,1)S(1)}, bf16[2048,128]{1,0:T(8,128)(2,1)S(1)}, u32[]{:S(2)}, u32[]{:S(2)}) collective-permute-start(bf16[2048,128]{1,0:T(8,128)(2,1)S(1)} %add_convert_fusion.4), channel_id=1, source_target_pairs={{0,14},{1,3},{2,0},{3,5},{4,2},{5,7},{6,4},{7,9},{8,6},{9,11},{10,... | collective-permute-start | bytes 1572872 | tf_op jit(solution)/shard_map/ppermute | solution.py:31
  102.0 1.0 shard_map.60.refs_4_
  103.0 2.8 %shard_map.61 = (f32[2048,128]{1,0:T(8,128)S(1)}, f32[2048,128]{1,0:T(8,128)S(1)}) custom-call(s32[1]{0:T(128)} %bitcast.core_ref, bf16[2048,128]{1,0:T(8,128)(2,1)S(1)} %collective-permute-done.1.refs_0_, bf16[2048,128]{1,0:T(8,128)(2,1)S(1)} %collective-permute-done.5.refs_1_, bf16[4,1088,512]{2,1,0:T(8,128)(2,1)S(1)} %get-tuple-element.23.refs_1_.refs_2_, ...), custom_call_target="tpu_custom_call" | custom-call | tf_op jit(solution)/shard_map/pallas_call | solution.py:241
  106.1 1.3 collective-permute-start.27
  107.4 4.2 %collective-permute-done.22 = bf16[2048,128]{1,0:T(8,128)(2,1)S(1)} collective-permute-done((bf16[2048,128]{1,0:T(8,128)(2,1)S(1)}, bf16[2048,128]{1,0:T(8,128)(2,1)S(1)}, u32[]{:S(2)}, u32[]{:S(2)}) %collective-permute-start.22) | collective-permute-done | bytes 524320 | tf_op jit(solution)/shard_map/ppermute | solution.py:31
  111.7 1.3 collective-permute-start.23
  113.0 1.0 shard_map.62.refs_3_
  114.0 2.4 %shard_map.63 = f32[2048,128]{1,0:T(8,128)S(1)} custom-call(s32[1]{0:T(128)} %bitcast.core_ref, bf16[2048,128]{1,0:T(8,128)(2,1)S(1)} %collective-permute-done.refs_0_, bf16[4,1088,512]{2,1,0:T(8,128)(2,1)S(1)} %get-tuple-element.23.refs_1_.refs_2_, bf16[4,1088,512]{2,1,0:T(8,128)(2,1)S(1)} %hold.5.refs_2_.refs_3_, bf16[352,128]{1,0:T(8,128)(2,1)S(1)} %shard_map.62.refs_3_), custom_call_target="tpu_custom_call" | custom-call | tf_op jit(solution)/shard_map/pallas_call | solution.py:241
  117.2 5.6 %collective-permute-done.23 = bf16[2048,128]{1,0:T(8,128)(2,1)S(1)} collective-permute-done((bf16[2048,128]{1,0:T(8,128)(2,1)S(1)}, bf16[2048,128]{1,0:T(8,128)(2,1)S(1)}, u32[]{:S(2)}, u32[]{:S(2)}) %collective-permute-start.23) | collective-permute-done | bytes 524320 | tf_op jit(solution)/shard_map/ppermute | solution.py:31
  122.9 1.3 collective-permute-start.24
  124.2 1.0 shard_map.55.refs_3_
  125.2 2.4 %shard_map.56.own = f32[2048,128]{1,0:T(8,128)S(1)} custom-call(s32[1]{0:T(128)} %bitcast.core_ref, bf16[2048,128]{1,0:T(8,128)(2,1)S(1)} %copy-done, bf16[4,1088,512]{2,1,0:T(8,128)(2,1)S(1)} %get-tuple-element.23.refs_1_.refs_2_, bf16[4,1088,512]{2,1,0:T(8,128)(2,1)S(1)} %hold.5.refs_2_.refs_3_, bf16[352,128]{1,0:T(8,128)(2,1)S(1)} %shard_map.55.refs_3_), custom_call_target="tpu_custom_call" | custom-call | tf_op jit(solution)/shard_map/pallas_call | solution.py:241
  127.6 4.6 %collective-permute-done.24.first = bf16[2048,128]{1,0:T(8,128)(2,1)S(1)} collective-permute-done((bf16[2048,128]{1,0:T(8,128)(2,1)S(1)}, bf16[2048,128]{1,0:T(8,128)(2,1)S(1)}, u32[]{:S(2)}, u32[]{:S(2)}) %collective-permute-start.24) | collective-permute-done | bytes 524320 | tf_op jit(solution)/shard_map/ppermute | solution.py:31
  132.2 1.0 close.1
  (67 shorter events, 9.0 us)
Async XLA Ops:
  2.7 18.1 %all-to-all-start = ((bf16[4,1088,128]{2,1,0:T(8,128)(2,1)}), bf16[4,1088,128]{2,1,0:T(8,128)(2,1)S(1)}, u32[]{:S(2)}, u32[]{:S(2)}) async-start(bf16[4,1088,128]{2,1,0:T(8,128)(2,1)} %get-tuple-element.19), calls=%async_computation | async-start | bytes 2228224 | tf_op jit(solution)/shard_map/all_to_all | solution.py:46
  8.4 12.3 %collective-permute-start = (bf16[2048,128]{1,0:T(8,128)(2,1)}, bf16[2048,128]{1,0:T(8,128)(2,1)S(1)}, u32[]{:S(2)}, u32[]{:S(2)}) collective-permute-start(bf16[2048,128]{1,0:T(8,128)(2,1)} %get-tuple-element.18.refs_0_), channel_id=1, source_target_pairs={{0,2},{1,15},{2,4},{3,1},{4,6},{5,3},{6,8},{7,5},{8,10},{9,7},{10,... | collective-permute-start | bytes 1572872 | tf_op jit(solution)/shard_map/ppermute | solution.py:31
  9.4 13.9 %collective-permute-start.4 = (bf16[2048,128]{1,0:T(8,128)(2,1)}, bf16[2048,128]{1,0:T(8,128)(2,1)S(1)}, u32[]{:S(2)}, u32[]{:S(2)}) collective-permute-start(bf16[2048,128]{1,0:T(8,128)(2,1)} %get-tuple-element.18.refs_0_), channel_id=1, source_target_pairs={{0,1},{1,0},{2,3},{3,2},{4,5},{5,4},{6,7},{7,6},{8,9},{9,8},{10,11... | collective-permute-start | bytes 1572872 | tf_op jit(solution)/shard_map/ppermute | solution.py:42
  20.7 10.4 %collective-permute-start.1 = (bf16[2048,128]{1,0:T(8,128)(2,1)S(1)}, bf16[2048,128]{1,0:T(8,128)(2,1)S(1)}, u32[]{:S(2)}, u32[]{:S(2)}) collective-permute-start(bf16[2048,128]{1,0:T(8,128)(2,1)S(1)} %collective-permute-done.refs_0_), channel_id=1, source_target_pairs={{0,2},{1,15},{2,4},{3,1},{4,6},{5,3},{6,8},{7,5},{8,10},{9,7},{10,... | collective-permute-start | bytes 1572872 | tf_op jit(solution)/shard_map/ppermute | solution.py:31
  21.0 35.5 %collective-permute-start.16 = (bf16[1088,512]{1,0:T(8,128)(2,1)S(1)}, bf16[1088,512]{1,0:T(8,128)(2,1)S(1)}, u32[]{:S(2)}, u32[]{:S(2)}) collective-permute-start(bf16[1088,512]{1,0:T(8,128)(2,1)S(1)} %get-tuple-element.22.refs_0_), channel_id=1, source_target_pairs={{0,1},{1,0},{2,3},{3,2},{4,5},{5,4},{6,7},{7,6},{8,9},{9,8},{10,11... | collective-permute-start | bytes 3342344 | tf_op jit(solution)/shard_map/ppermute | solution.py:42
  22.2 1.0 copy-start.3
  23.3 13.5 %collective-permute-start.5 = (bf16[2048,128]{1,0:T(8,128)(2,1)S(1)}, bf16[2048,128]{1,0:T(8,128)(2,1)S(1)}, u32[]{:S(2)}, u32[]{:S(2)}) collective-permute-start(bf16[2048,128]{1,0:T(8,128)(2,1)S(1)} %collective-permute-done.4), channel_id=1, source_target_pairs={{0,2},{1,15},{2,4},{3,1},{4,6},{5,3},{6,8},{7,5},{8,10},{9,7},{10,... | collective-permute-start | bytes 1572872 | tf_op jit(solution)/shard_map/ppermute | solution.py:31
  23.3 16.5 %collective-permute-start.10 = (bf16[544,512]{1,0:T(8,128)(2,1)S(1)}, bf16[544,512]{1,0:T(8,128)(2,1)S(1)}, u32[]{:S(2)}, u32[]{:S(2)}) collective-permute-start(bf16[544,512]{1,0:T(8,128)(2,1)S(1)} %get-tuple-element.21), channel_id=1, source_target_pairs={{0,192},{16,208},{32,224},{48,240},{64,0},{80,16},{96,32},{112,48}... | collective-permute-start | bytes 1671176 | tf_op jit(solution)/shard_map/ppermute | solution.py:38
  26.2 13.5 %collective-permute-start.8 = (bf16[544,512]{1,0:T(8,128)(2,1)S(1)}, bf16[544,512]{1,0:T(8,128)(2,1)S(1)}, u32[]{:S(2)}, u32[]{:S(2)}) collective-permute-start(bf16[544,512]{1,0:T(8,128)(2,1)S(1)} %get-tuple-element.20), channel_id=1, source_target_pairs={{0,64},{16,80},{32,96},{48,112},{64,128},{80,144},{96,160},{112,17... | collective-permute-start | bytes 1671176 | tf_op jit(solution)/shard_map/ppermute | solution.py:38
  31.1 11.8 %collective-permute-start.12 = (bf16[544,512]{1,0:T(8,128)(2,1)S(1)}, bf16[544,512]{1,0:T(8,128)(2,1)S(1)}, u32[]{:S(2)}, u32[]{:S(2)}) collective-permute-start(bf16[544,512]{1,0:T(8,128)(2,1)S(1)} %get-tuple-element.21), channel_id=1, source_target_pairs={{0,64},{16,80},{32,96},{48,112},{64,128},{80,144},{96,160},{112,17... | collective-permute-start | bytes 1671176 | tf_op jit(solution)/shard_map/ppermute | solution.py:38
  36.7 10.1 %collective-permute-start.13 = (bf16[544,512]{1,0:T(8,128)(2,1)S(1)}, bf16[544,512]{1,0:T(8,128)(2,1)}, u32[]{:S(2)}, u32[]{:S(2)}) collective-permute-start(bf16[544,512]{1,0:T(8,128)(2,1)S(1)} %get-tuple-element.20), channel_id=1, source_target_pairs={{0,192},{16,208},{32,224},{48,240},{64,0},{80,16},{96,32},{112,48}... | collective-permute-start | bytes 1671176 | tf_op jit(solution)/shard_map/ppermute | solution.py:38
  39.7 10.4 %collective-permute-start.2 = (bf16[2048,128]{1,0:T(8,128)(2,1)S(1)}, bf16[2048,128]{1,0:T(8,128)(2,1)S(1)}, u32[]{:S(2)}, u32[]{:S(2)}) collective-permute-start(bf16[2048,128]{1,0:T(8,128)(2,1)S(1)} %collective-permute-done.1.refs_0_), channel_id=1, source_target_pairs={{0,2},{1,15},{2,4},{3,1},{4,6},{5,3},{6,8},{7,5},{8,10},{9,7},{10,... | collective-permute-start | bytes 1572872 | tf_op jit(solution)/shard_map/ppermute | solution.py:31
  39.8 16.0 %collective-permute-start.6 = (bf16[2048,128]{1,0:T(8,128)(2,1)S(1)}, bf16[2048,128]{1,0:T(8,128)(2,1)S(1)}, u32[]{:S(2)}, u32[]{:S(2)}) collective-permute-start(bf16[2048,128]{1,0:T(8,128)(2,1)S(1)} %collective-permute-done.5.refs_1_), channel_id=1, source_target_pairs={{0,2},{1,15},{2,4},{3,1},{4,6},{5,3},{6,8},{7,5},{8,10},{9,7},{10,... | collective-permute-start | bytes 1572872 | tf_op jit(solution)/shard_map/ppermute | solution.py:31
  42.9 15.9 %collective-permute-start.11 = (bf16[544,512]{1,0:T(8,128)(2,1)S(1)}, bf16[544,512]{1,0:T(8,128)(2,1)}, u32[]{:S(2)}, u32[]{:S(2)}) collective-permute-start(bf16[544,512]{1,0:T(8,128)(2,1)S(1)} %collective-permute-done.10.refs_4_), channel_id=1, source_target_pairs={{0,192},{16,208},{32,224},{48,240},{64,0},{80,16},{96,32},{112,48}... | collective-permute-start | bytes 1671176 | tf_op jit(solution)/shard_map/ppermute | solution.py:38
  46.8 12.1 %collective-permute-start.9 = (bf16[544,512]{1,0:T(8,128)(2,1)S(1)}, bf16[544,512]{1,0:T(8,128)(2,1)}, u32[]{:S(2)}, u32[]{:S(2)}) collective-permute-start(bf16[544,512]{1,0:T(8,128)(2,1)S(1)} %collective-permute-done.8.refs_1_), channel_id=1, source_target_pairs={{0,64},{16,80},{32,96},{48,112},{64,128},{80,144},{96,160},{112,17... | collective-permute-start | bytes 1671176 | tf_op jit(solution)/shard_map/ppermute | solution.py:38
  50.1 9.3 %collective-permute-start.17 = (bf16[544,512]{1,0:T(8,128)(2,1)S(1)}, bf16[544,512]{1,0:T(8,128)(2,1)S(1)}, u32[]{:S(2)}, u32[]{:S(2)}) collective-permute-start(bf16[544,512]{1,0:T(8,128)(2,1)S(1)} %collective-permute-done.8.refs_1_), channel_id=1, source_target_pairs={{0,1},{1,0},{2,3},{3,2},{4,5},{5,4},{6,7},{7,6},{8,9},{9,8},{10,11... | collective-permute-start | bytes 1671176 | tf_op jit(solution)/shard_map/ppermute | solution.py:42
  50.1 0.8 copy-start.7
  55.8 4.6 %collective-permute-start.20 = (bf16[544,512]{1,0:T(8,128)(2,1)S(1)}, bf16[544,512]{1,0:T(8,128)(2,1)S(1)}, u32[]{:S(2)}, u32[]{:S(2)}) collective-permute-start(bf16[544,512]{1,0:T(8,128)(2,1)S(1)} %collective-permute-done.10.refs_4_), channel_id=1, source_target_pairs={{0,1},{1,0},{2,3},{3,2},{4,5},{5,4},{6,7},{7,6},{8,9},{9,8},{10,11... | collective-permute-start | bytes 1671176 | tf_op jit(solution)/shard_map/ppermute | solution.py:42
  55.8 0.8 copy-start.5
  56.6 1.0 copy-start.1
  57.6 3.6 %collective-permute-start.18 = (bf16[544,512]{1,0:T(8,128)(2,1)S(1)}, bf16[544,512]{1,0:T(8,128)(2,1)S(1)}, u32[]{:S(2)}, u32[]{:S(2)}) collective-permute-start(bf16[544,512]{1,0:T(8,128)(2,1)S(1)} %collective-permute-done.12.refs_2_), channel_id=1, source_target_pairs={{0,1},{1,0},{2,3},{3,2},{4,5},{5,4},{6,7},{7,6},{8,9},{9,8},{10,11... | collective-permute-start | bytes 1671176 | tf_op jit(solution)/shard_map/ppermute | solution.py:42
  58.1 0.8 copy-start.9
  58.9 9.3 %collective-permute-start.19 = (bf16[544,512]{1,0:T(8,128)(2,1)}, bf16[544,512]{1,0:T(8,128)(2,1)}, u32[]{:S(2)}, u32[]{:S(2)}) collective-permute-start(bf16[544,512]{1,0:T(8,128)(2,1)} %collective-permute-done.13.refs_3_), channel_id=1, source_target_pairs={{0,1},{1,0},{2,3},{3,2},{4,5},{5,4},{6,7},{7,6},{8,9},{9,8},{10,11... | collective-permute-start | bytes 1671176 | tf_op jit(solution)/shard_map/ppermute | solution.py:42
  58.9 21.4 %collective-permute-start.14 = (bf16[544,512]{1,0:T(8,128)(2,1)}, bf16[544,512]{1,0:T(8,128)(2,1)}, u32[]{:S(2)}, u32[]{:S(2)}) collective-permute-start(bf16[544,512]{1,0:T(8,128)(2,1)} %collective-permute-done.9.refs_2_), channel_id=1, source_target_pairs={{0,1},{1,0},{2,3},{3,2},{4,5},{5,4},{6,7},{7,6},{8,9},{9,8},{10,11... | collective-permute-start | bytes 1671176 | tf_op jit(solution)/shard_map/ppermute | solution.py:42
  59.4 0.9 copy-start.11
  60.3 20.1 %collective-permute-start.15 = (bf16[544,512]{1,0:T(8,128)(2,1)}, bf16[544,512]{1,0:T(8,128)(2,1)}, u32[]{:S(2)}, u32[]{:S(2)}) collective-permute-start(bf16[544,512]{1,0:T(8,128)(2,1)} %collective-permute-done.11.refs_3_), channel_id=1, source_target_pairs={{0,1},{1,0},{2,3},{3,2},{4,5},{5,4},{6,7},{7,6},{8,9},{9,8},{10,11... | collective-permute-start | bytes 1671176 | tf_op jit(solution)/shard_map/ppermute | solution.py:42
  60.4 0.8 copy-start.13
  61.2 10.4 %collective-permute-start.3 = (bf16[2048,128]{1,0:T(8,128)(2,1)S(1)}, bf16[2048,128]{1,0:T(8,128)(2,1)S(1)}, u32[]{:S(2)}, u32[]{:S(2)}) collective-permute-start(bf16[2048,128]{1,0:T(8,128)(2,1)S(1)} %collective-permute-done.2.refs_0_), channel_id=1, source_target_pairs={{0,2},{1,15},{2,4},{3,1},{4,6},{5,3},{6,8},{7,5},{8,10},{9,7},{10,... | collective-permute-start | bytes 1572872 | tf_op jit(solution)/shard_map/ppermute | solution.py:31
  61.2 0.9 copy-start.15
  62.1 15.3 %collective-permute-start.7 = (bf16[2048,128]{1,0:T(8,128)(2,1)S(1)}, bf16[2048,128]{1,0:T(8,128)(2,1)}, u32[]{:S(2)}, u32[]{:S(2)}) collective-permute-start(bf16[2048,128]{1,0:T(8,128)(2,1)S(1)} %collective-permute-done.6.refs_1_), channel_id=1, source_target_pairs={{0,2},{1,15},{2,4},{3,1},{4,6},{5,3},{6,8},{7,5},{8,10},{9,7},{10,... | collective-permute-start | bytes 1572872 | tf_op jit(solution)/shard_map/ppermute | solution.py:31
  62.1 6.1 %copy-start.2 = (bf16[1088,512]{1,0:T(8,128)(2,1)S(1)}, bf16[1088,512]{1,0:T(8,128)(2,1)}, u32[]{:S(2)}) copy-start(bf16[1088,512]{1,0:T(8,128)(2,1)} %copy-done.1) | copy-start | bytes 3342340
  62.1 1.3 %copy-start.4 = (bf16[1088,512]{1,0:T(8,128)(2,1)S(1)}, bf16[1088,512]{1,0:T(8,128)(2,1)}, u32[]{:S(2)}) copy-start(bf16[1088,512]{1,0:T(8,128)(2,1)} %copy-done.3) | copy-start | bytes 3342340
  63.4 1.1 copy-start.6
  64.5 1.1 copy-start.8
  65.5 1.1 copy-start.10
  66.6 1.6 %copy-start.12 = (bf16[544,512]{1,0:T(8,128)(2,1)S(1)}, bf16[544,512]{1,0:T(8,128)(2,1)}, u32[]{:S(2)}) copy-start(bf16[544,512]{1,0:T(8,128)(2,1)} %copy-done.11) | copy-start | bytes 1671172
  66.6 1.6 %copy-start.14 = (bf16[544,512]{1,0:T(8,128)(2,1)S(1)}, bf16[544,512]{1,0:T(8,128)(2,1)}, u32[]{:S(2)}) copy-start(bf16[544,512]{1,0:T(8,128)(2,1)} %copy-done.13) | copy-start | bytes 1671172
  66.6 1.6 %copy-start.16 = (bf16[544,512]{1,0:T(8,128)(2,1)S(1)}, bf16[544,512]{1,0:T(8,128)(2,1)}, u32[]{:S(2)}) copy-start(bf16[544,512]{1,0:T(8,128)(2,1)} %copy-done.15) | copy-start | bytes 1671172
  85.5 9.3 %collective-permute-start.25 = (bf16[2048,128]{1,0:T(8,128)(2,1)S(1)}, bf16[2048,128]{1,0:T(8,128)(2,1)S(1)}, u32[]{:S(2)}, u32[]{:S(2)}) collective-permute-start(bf16[2048,128]{1,0:T(8,128)(2,1)S(1)} %get-tuple-element.28), channel_id=1, source_target_pairs={{0,14},{1,3},{2,0},{3,5},{4,2},{5,7},{6,4},{7,9},{8,6},{9,11},{10,... | collective-permute-start | bytes 1572872 | tf_op jit(solution)/shard_map/ppermute | solution.py:31
  85.5 14.8 %collective-permute-start.21 = (bf16[2048,128]{1,0:T(8,128)(2,1)S(1)}, bf16[2048,128]{1,0:T(8,128)(2,1)S(1)}, u32[]{:S(2)}, u32[]{:S(2)}) collective-permute-start(bf16[2048,128]{1,0:T(8,128)(2,1)S(1)} %get-tuple-element.25), channel_id=1, source_target_pairs={{0,14},{1,3},{2,0},{3,5},{4,2},{5,7},{6,4},{7,9},{8,6},{9,11},{10,... | collective-permute-start | bytes 1572872 | tf_op jit(solution)/shard_map/ppermute | solution.py:31
  94.9 11.1 %collective-permute-start.26 = (bf16[2048,128]{1,0:T(8,128)(2,1)S(1)}, bf16[2048,128]{1,0:T(8,128)(2,1)S(1)}, u32[]{:S(2)}, u32[]{:S(2)}) collective-permute-start(bf16[2048,128]{1,0:T(8,128)(2,1)S(1)} %add_convert_fusion.1), channel_id=1, source_target_pairs={{0,14},{1,3},{2,0},{3,5},{4,2},{5,7},{6,4},{7,9},{8,6},{9,11},{10,... | collective-permute-start | bytes 1572872 | tf_op jit(solution)/shard_map/ppermute | solution.py:31
  100.5 11.1 %collective-permute-start.22 = (bf16[2048,128]{1,0:T(8,128)(2,1)S(1)}, bf16[2048,128]{1,0:T(8,128)(2,1)S(1)}, u32[]{:S(2)}, u32[]{:S(2)}) collective-permute-start(bf16[2048,128]{1,0:T(8,128)(2,1)S(1)} %add_convert_fusion.4), channel_id=1, source_target_pairs={{0,14},{1,3},{2,0},{3,5},{4,2},{5,7},{6,4},{7,9},{8,6},{9,11},{10,... | collective-permute-start | bytes 1572872 | tf_op jit(solution)/shard_map/ppermute | solution.py:31
  106.1 11.1 %collective-permute-start.27 = (bf16[2048,128]{1,0:T(8,128)(2,1)S(1)}, bf16[2048,128]{1,0:T(8,128)(2,1)S(1)}, u32[]{:S(2)}, u32[]{:S(2)}) collective-permute-start(bf16[2048,128]{1,0:T(8,128)(2,1)S(1)} %add_convert_fusion), channel_id=1, source_target_pairs={{0,14},{1,3},{2,0},{3,5},{4,2},{5,7},{6,4},{7,9},{8,6},{9,11},{10,... | collective-permute-start | bytes 1572872 | tf_op jit(solution)/shard_map/ppermute | solution.py:31
  111.7 11.1 %collective-permute-start.23 = (bf16[2048,128]{1,0:T(8,128)(2,1)S(1)}, bf16[2048,128]{1,0:T(8,128)(2,1)S(1)}, u32[]{:S(2)}, u32[]{:S(2)}) collective-permute-start(bf16[2048,128]{1,0:T(8,128)(2,1)S(1)} %add_convert_fusion.3), channel_id=1, source_target_pairs={{0,14},{1,3},{2,0},{3,5},{4,2},{5,7},{6,4},{7,9},{8,6},{9,11},{10,... | collective-permute-start | bytes 1572872 | tf_op jit(solution)/shard_map/ppermute | solution.py:31
  114.0 10.3 %copy-start = (bf16[2048,128]{1,0:T(8,128)(2,1)S(1)}, bf16[2048,128]{1,0:T(8,128)(2,1)}, u32[]{:S(2)}) copy-start(bf16[2048,128]{1,0:T(8,128)(2,1)} %get-tuple-element.18.refs_0_) | copy-start | bytes 1572868
  117.2 10.4 %collective-permute-start.28 = (bf16[2048,128]{1,0:T(8,128)(2,1)S(1)}, bf16[2048,128]{1,0:T(8,128)(2,1)S(1)}, u32[]{:S(2)}, u32[]{:S(2)}) collective-permute-start(bf16[2048,128]{1,0:T(8,128)(2,1)S(1)} %collective-permute-done.27), channel_id=1, source_target_pairs={{0,1},{1,0},{2,3},{3,2},{4,5},{5,4},{6,7},{7,6},{8,9},{9,8},{10,11... | collective-permute-start | bytes 1572872 | tf_op jit(solution)/shard_map/ppermute | solution.py:42
  122.9 9.3 %collective-permute-start.24 = (bf16[2048,128]{1,0:T(8,128)(2,1)S(1)}, bf16[2048,128]{1,0:T(8,128)(2,1)S(1)}, u32[]{:S(2)}, u32[]{:S(2)}) collective-permute-start(bf16[2048,128]{1,0:T(8,128)(2,1)S(1)} %add_convert_fusion.2), channel_id=1, source_target_pairs={{0,14},{1,3},{2,0},{3,5},{4,2},{5,7},{6,4},{7,9},{8,6},{9,11},{10,... | collective-permute-start | bytes 1572872 | tf_op jit(solution)/shard_map/ppermute | solution.py:31
